TPU v7x, 32 devices: a whole 2x2x4 slice. The times are simulated.
32 devices in a mesh: grp: 2 (over y), kv: 4 (over z), tp: 4 (over x, core).
Axes of the slice: x: 2, y: 2, z: 4, core: 2. Of those that a mesh axis runs over, the one named last changes fastest.
Arguments:
- candidate_embeddings: bfloat16 [1536, 4096], P(('grp', 'kv'), 'tp'), parts along dimension 0, may hold values from -100 to 100
- incoming_rms_scaling: float32 [4096], replicated, may hold values from 0.1 to 1.9
- probe_projector: bfloat16 [4096, 2048], P('kv', 'tp'), may hold values from -0.09375 to 0.09375
- address_projector: bfloat16 [4096, 2048], P('kv', 'tp'), may hold values from -0.09375 to 0.09375
- content_projector: bfloat16 [4096, 2048], P('kv', 'tp'), may hold values from -0.09375 to 0.09375
- sigmoid_mask_matrix: bfloat16 [4096, 2048], P('kv', 'tp'), may hold values from -0.09375 to 0.09375
- forgetting_projector: bfloat16 [4096, 16], replicated, may hold values from -0.09375 to 0.09375
- strength_projector_matrix: bfloat16 [4096, 16], replicated, may hold values from -0.09375 to 0.09375
- channel_forgetting_rates: float32 [16], P('tp'), may hold values from -3 to 0.5
- forgetting_offset: float32 [16], P('tp'), may hold values from -1 to 1
- extra_forgetting: float32 [384, 4, 16], P(('grp', 'kv'), None, 'tp'), parts along dimension 0, may hold values from -0.7 to 0, as said below
- outgoing_rms_scaling: float32 [128], replicated, may hold values from 0.1 to 1.9
- final_projector: bfloat16 [2048, 4096], P('tp', 'kv'), may hold values from -0.125 to 0.125
- memory_matrix: float32 [384, 16, 128, 128], P(('grp', 'kv'), 'tp'), parts along dimension 0, may hold values from -4 to 4
- earlier_addresses: bfloat16 [384, 4, 16, 128], P(('grp', 'kv'), None, 'tp'), parts along dimension 0, may hold values from -6 to 6
- earlier_contents: bfloat16 [384, 4, 16, 128], P(('grp', 'kv'), None, 'tp'), parts along dimension 0, may hold values from -6 to 6
- earlier_strengths: float32 [384, 4, 16], P(('grp', 'kv'), None, 'tp'), parts along dimension 0, may hold values from 0.1 to 0.9
- earlier_forgetting: float32 [384, 4, 16], P(('grp', 'kv'), None, 'tp'), parts along dimension 0, may hold values from -1.5 to -0.02
- admitted_counts: int32 [384], P(('grp', 'kv')), parts along dimension 0, may hold values from 0 to 4
Outputs:
- mixed: bfloat16 [1536, 4096], P(('grp', 'kv'), 'tp'), parts along dimension 0
- taken_state: float32 [384, 16, 128, 128], P(('grp', 'kv'), 'tp'), parts along dimension 0
There are 2 independent parts, one for each index of `grp`. A program takes and returns all parts, laid end to end along the dimension named above; an argument that names none is the same for every part. Nothing has to cross between parts.
Inputs may be any that keep to these rules, and one draw needn't show every extreme that they name: `extra_forgetting`: mostly zero; elsewhere the logarithm of a factor between 0.5 and 0.8.
All inputs are finite; a program needn't handle non-finite values.
Results may differ from a plain program's by a relative error of at most 0.015.
Values may be sent and summed in bfloat16 or wider, within the bound.
A program may use at most 128 MiB of HBM per device.

v0:
```python
import functools

import jax
import jax.numpy as jnp
from jax import lax
from jax.experimental import pallas as pl
from jax.experimental.pallas import tpu as pltpu
from jax.sharding import PartitionSpec as P

DK = 128
P_SIZE = 4
SB = 8
TALL = SB * P_SIZE
epsilon = 1e-06
f32 = jnp.float32
bf16 = jnp.bfloat16


def lane_dot(a, b):
    return jnp.sum(a * b, axis=-1, keepdims=True)


def first_half():
    return lax.broadcasted_iota(jnp.int32, (8, DK), 0) < P_SIZE


def load_heads(heads, src, dst, factor=None):
    for h in range(heads):
        part = src[:, h * DK : (h + 1) * DK].astype(f32)
        dst[pl.ds(h * TALL, TALL), :] = part if factor is None else (part * factor).astype(bf16).astype(f32)


def tile(h, pair):
    return pl.ds(h * TALL + pair * 8, 8)


def proposal(h, p):
    return pl.ds(h * TALL + p, SB, stride=P_SIZE)


def accepted_kernel(heads, s_ref, k_ref, v_ref, n_ref, o_ref, r_scr, u_scr, c_scr, kf, vf):
    load_heads(heads, k_ref, kf)
    load_heads(heads, v_ref, vf)
    low = first_half()
    for pair in range(SB // 2):
        for h in range(heads):
            at = tile(h, pair)
            lhs = kf[at, :].astype(bf16)
            r0 = jnp.dot(lhs, s_ref[2 * pair, h].astype(bf16), preferred_element_type=f32)
            r1 = jnp.dot(lhs, s_ref[2 * pair + 1, h].astype(bf16), preferred_element_type=f32)
            r_scr[at, :] = jnp.where(low, r0, r1)
    few = n_ref[...]
    span = P_SIZE * heads
    count = few[:, 2 * span : 2 * span + 1]
    for h in range(heads):
        scale = jnp.ones((SB, 1), f32)
        ks, us, norms = [], [], []
        for p in range(P_SIZE):
            at = proposal(h, p)
            col = slice(p * heads + h, p * heads + h + 1)
            key = kf[at, :]
            norm = lax.rsqrt(lane_dot(key, key) + epsilon)
            live = count > float(p)
            g = jnp.where(live, jnp.exp(few[:, p * heads + h : p * heads + h + 1]), 1.0)
            b = jnp.where(live, few[:, span + p * heads + h : span + p * heads + h + 1], 0.0)
            rec = (scale * norm) * r_scr[at, :]
            for ki, ui, ni in zip(ks, us, norms):
                rec = rec + (lane_dot(ki, key) * (ni * norm)) * ui
            us = [ui * g for ui in us]
            scale = scale * g
            us.append(b * (vf[at, :] - g * rec))
            ks.append(key)
            norms.append(norm)
        for p in range(P_SIZE):
            u_scr[proposal(h, p), :] = us[p] * norms[p]
        c_scr[pl.ds(h * SB, SB), :] = jnp.broadcast_to(scale, (SB, DK))
    for pair in range(SB // 2):
        for h in range(heads):
            at = tile(h, pair)
            key = kf[at, :]
            lhs = jnp.concatenate([key, key], axis=0).astype(bf16)
            u = u_scr[at, :]
            hi = u.astype(bf16).astype(f32)
            lo = u - hi
            for half in range(2):
                keep = low if half == 0 else jnp.logical_not(low)
                rhs = jnp.concatenate([jnp.where(keep, hi, 0.0), jnp.where(keep, lo, 0.0)], axis=0).astype(bf16)
                seq = 2 * pair + half
                add = lax.dot_general(lhs, rhs, (((0,), (0,)), ((), ())), preferred_element_type=f32)
                o_ref[seq, h] = c_scr[pl.ds(h * SB + seq, 1), :] * s_ref[seq, h] + add


def attend_kernel(heads, s_ref, a_ref, q_ref, k_ref, v_ref, z_ref, d_ref, b_ref, w_ref, o_ref, kept, rk, rq, qf, kf, vf, zf, of, done):
    keep = pltpu.make_async_copy(s_ref, kept.at[pl.ds(pl.program_id(0) * SB, SB)], done)
    keep.start()
    for src, dst in ((q_ref, qf), (k_ref, kf), (v_ref, vf), (z_ref, zf)):
        load_heads(heads, src, dst, a_ref[...])
    low = first_half()
    for pair in range(SB // 2):
        for h in range(heads):
            at = tile(h, pair)
            lhs = jnp.concatenate([kf[at, :], qf[at, :]], axis=0).astype(bf16)
            r0 = jnp.dot(lhs, s_ref[2 * pair, h].astype(bf16), preferred_element_type=f32)
            r1 = jnp.dot(lhs, s_ref[2 * pair + 1, h].astype(bf16), preferred_element_type=f32)
            rk[at, :] = jnp.where(low, r0[:8], r1[:8])
            rq[at, :] = jnp.where(low, r0[8:], r1[8:])
    gain = w_ref[...]
    for h in range(heads):
        scale = jnp.ones((SB, 1), f32)
        ks, us, norms = [], [], []
        for p in range(P_SIZE):
            at = proposal(h, p)
            col = slice(p * heads + h, p * heads + h + 1)
            key = kf[at, :]
            query = qf[at, :]
            norm = lax.rsqrt(lane_dot(key, key) + epsilon)
            qnorm = lax.rsqrt(lane_dot(query, query) + epsilon) * DK ** (-0.5)
            g = jnp.exp(d_ref[:, col])
            rec = (scale * norm) * rk[at, :]
            for ki, ui, ni in zip(ks, us, norms):
                rec = rec + (lane_dot(ki, key) * (ni * norm)) * ui
            us = [ui * g for ui in us]
            scale = scale * g
            us.append(b_ref[:, col] * (vf[at, :] - g * rec))
            ks.append(key)
            norms.append(norm)
            att = (scale * qnorm) * rq[at, :]
            for ki, ui, ni in zip(ks, us, norms):
                att = att + (lane_dot(ki, query) * (ni * qnorm)) * ui
            gate = zf[at, :]
            mean = jnp.sum(att * att, axis=-1, keepdims=True) / DK
            of[at, :] = att * lax.rsqrt(mean + epsilon) * gain * (gate * jax.nn.sigmoid(gate))
    for h in range(heads):
        o_ref[:, h * DK : (h + 1) * DK] = of[pl.ds(h * TALL, TALL), :].astype(bf16)
    keep.wait()


def accepted(state, keys, values, few):
    seqs, heads = state.shape[:2]
    width = heads * DK
    rows = TALL
    tall = pl.BlockSpec((rows, width), lambda i: (i, 0))
    thin = pl.BlockSpec((SB, few.shape[1]), lambda i: (i, 0))
    block = pl.BlockSpec((SB, heads, DK, DK), lambda i: (i, 0, 0, 0))
    return pl.pallas_call(
        functools.partial(accepted_kernel, heads),
        grid=(seqs // SB,),
        in_specs=[block, tall, tall, thin],
        out_specs=block,
        out_shape=jax.ShapeDtypeStruct(state.shape, f32),
        scratch_shapes=[pltpu.VMEM((heads * n, DK), f32) for n in (TALL, TALL, SB, TALL, TALL)],
        cost_estimate=pl.CostEstimate(flops=10_000_000_000, bytes_accessed=2 * state.size * 4, transcendentals=0),
        name="accepted",
    )(state, keys, values, few)


def attend(state, packed, factor, decay, beta, gain):
    seqs, heads = state.shape[:2]
    width = heads * DK
    rows = TALL
    thin = pl.BlockSpec((SB, P_SIZE * heads), lambda i: (i, 0))
    block = pl.BlockSpec((SB, heads, DK, DK), lambda i: (i, 0, 0, 0))

    def part(n):
        return pl.BlockSpec((rows, width), lambda i: (i, n))

    return pl.pallas_call(
        functools.partial(attend_kernel, heads),
        grid=(seqs // SB,),
        in_specs=[block, pl.BlockSpec((rows, 1), lambda i: (i, 0)), part(0), part(1), part(2), part(3), thin, thin, pl.BlockSpec((1, DK), lambda i: (0, 0))],
        out_specs=[pl.BlockSpec((rows, width), lambda i: (i, 0)), pl.BlockSpec(memory_space=pl.ANY)],
        out_shape=[jax.ShapeDtypeStruct((seqs * P_SIZE, width), bf16), jax.ShapeDtypeStruct(state.shape, f32)],
        scratch_shapes=[pltpu.VMEM((heads * TALL, DK), f32)] * 7 + [pltpu.SemaphoreType.DMA],
        cost_estimate=pl.CostEstimate(flops=5_000_000_000, bytes_accessed=state.size * 4, transcendentals=0),
        name="attend",
    )(state, factor, packed, packed, packed, packed, decay, beta, gain.reshape(1, DK))


def pick(index, values):
    chosen = values[-1]
    for at, value in enumerate(values[:-1]):
        chosen = jnp.where(index == at, value, chosen)
    return chosen


def turned_slot(t):
    return pick(t, (0, 2, 1, 3))


ORDER = ((3, 2, 1, 0), (0, 2, 1, 3), (3, 1, 2, 0), (0, 1, 2, 3))


def project_kernel(x_ref, gain_ref, keys, values, thin, wq, wk, wv, wz, wf, ws, state, acc, few_ref, taken, xbuf, w, fs,
                   send, recv, esend, erecv, s_in, s_out, r_scr, u_scr, c_scr, kf, vf,
                   xs, xr, wsem, ps, pr, es, er, ins, outs):
    k, t, g = lax.axis_index("kv"), lax.axis_index("tp"), lax.axis_index("grp")
    depth, width = w.shape[1], w.shape[2]
    rows = x_ref.shape[0]

    def at(kv, tp):
        return {"grp": g, "kv": kv, "tp": tp}

    def remote(src, dst, ss, rs, kv, tp):
        return pltpu.make_async_remote_copy(src, dst, ss, rs, device_id=at(kv, tp), device_id_type=pl.DeviceIdType.MESH)

    loads = [pltpu.make_async_copy(src, w.at[i], wsem.at[i]) for i, src in enumerate((wq, wk, wv, wz))]
    here = pl.ds(k * depth, depth)
    loads += [pltpu.make_async_copy(src.at[:, here], fs.at[i], wsem.at[4 + i]) for i, src in enumerate((wf, ws))]
    slot = turned_slot(t)
    far_t, far_k = turned_slot(k), t
    home = jnp.logical_and(far_k == k, far_t == t)
    first = remote(x_ref, xbuf.at[k], xs.at[0], xr.at[k], far_k, far_t)
    local = pltpu.make_async_copy(x_ref, xbuf.at[k], xr.at[k])

    @pl.when(jnp.logical_not(home))
    def _():
        first.start()

    @pl.when(home)
    def _():
        local.start()

    for load in loads:
        load.start()

    beside = t + 1 - 2 * (t % 2)
    across = (t + 2) % 4

    def arrived(s):
        remote(xbuf.at[s], xbuf.at[s], xs.at[0], xr.at[s], k, beside).wait_recv()

    @pl.when(home)
    def _():
        local.wait()

    @pl.when(jnp.logical_not(home))
    def _():
        arrived(slot)

    over = remote(xbuf.at[slot], xbuf.at[slot], xs.at[1], xr.at[slot], k, across)
    over.start()
    near = remote(xbuf.at[slot], xbuf.at[slot], xs.at[2], xr.at[slot], k, beside)
    near.start()
    other = turned_slot(across)
    arrived(other)
    onward = remote(xbuf.at[other], xbuf.at[other], xs.at[3], xr.at[other], k, beside)
    onward.start()
    arrived(turned_slot(beside))
    arrived(turned_slot((beside + 2) % 4))
    for load in loads:
        load.wait()

    def step(i, carry):
        r = pick(k, [pick(i, row) for row in ORDER])
        own = r == k
        floated = xbuf[r].astype(f32)
        gained = (floated * gain_ref[k]).astype(bf16)
        squares = floated * floated
        high = squares.astype(bf16)
        rest = (squares - high.astype(f32)).astype(bf16)
        ones = jnp.ones((8, depth), bf16)
        nt = (((1,), (1,)), ((), ()))
        esend[r, 0:16, :] = lax.dot_general(fs[0], gained, nt, preferred_element_type=f32)
        esend[r, 16:32, :] = lax.dot_general(fs[1], gained, nt, preferred_element_type=f32)
        esend[r, 32:40, :] = lax.dot_general(ones, high, nt, preferred_element_type=f32) + lax.dot_general(
            ones, rest, nt, preferred_element_type=f32
        )
        for j in range(4):
            part = jnp.dot(gained, w[j], preferred_element_type=f32)
            cols = slice(j * width, (j + 1) * width)

            @pl.when(own)
            def _():
                acc[:, cols] = part

            @pl.when(jnp.logical_not(own))
            def _():
                send[r, :, cols] = part.astype(bf16)

        relayed = jnp.logical_or(jnp.logical_and(k == 1, r == 3), jnp.logical_and(k == 2, r == 0))

        @pl.when(relayed)
        def _():
            remote(send.at[r], recv.at[4], ps.at[r], pr.at[4], k, beside).wait_recv()

            def add(c, carry):
                at_rows = pl.ds(c * 16, 16)
                send[r, at_rows, :] = (send[r, at_rows, :].astype(f32) + recv[4, at_rows, :].astype(f32)).astype(bf16)
                return carry

            lax.fori_loop(0, rows // 16, add, 0)

        @pl.when(jnp.logical_not(own))
        def _():
            ends = jnp.logical_or(jnp.logical_and(k == 0, r == 3), jnp.logical_and(k == 3, r == 0))
            target = jnp.where(ends, jnp.where(k == 0, 1, 2), r)
            place = jnp.where(ends, 4, k)
            remote(send.at[r], recv.at[place], ps.at[r], pr.at[place], target, t).start()
            remote(esend.at[r], erecv.at[k], es.at[r], er.at[k], r, t).start()

        return carry

    lax.fori_loop(0, 3, step, 0)

    blocks = state.shape[0] // SB
    heads = state.shape[1]

    def fetch(i):
        return pltpu.make_async_copy(state.at[pl.ds(i * SB, SB)], s_in.at[i % 2], ins.at[i % 2])

    def put(i):
        return pltpu.make_async_copy(s_out.at[i % 2], taken.at[pl.ds(i * SB, SB)], outs.at[i % 2])

    def accept(i, carry):
        @pl.when(i + 1 < blocks)
        def _():
            fetch(i + 1).start()

        fetch(i).wait()

        @pl.when(i >= 2)
        def _():
            put(i - 2).wait()

        tall, few_rows = pl.ds(i * TALL, TALL), pl.ds(i * SB, SB)
        accepted_kernel(
            heads, s_in.at[i % 2], keys.at[tall], values.at[tall], thin.at[few_rows], s_out.at[i % 2],
            r_scr, u_scr, c_scr, kf, vf,
        )
        put(i).start()
        return carry

    fetch(0).start()
    lax.fori_loop(0, blocks, accept, 0)
    lax.fori_loop(3, 4, step, 0)
    for i in range(max(blocks - 2, 0), blocks):
        put(i).wait()

    first_wait = jnp.logical_not(home)

    @pl.when(first_wait)
    def _():
        first.wait_send()

    over.wait_send()
    near.wait_send()
    onward.wait_send()

    few_ref[...] = esend[k]
    for src in range(4):

        @pl.when(k != src)
        def _():
            remote(esend.at[src], erecv.at[src], es.at[src], er.at[src], k, beside).wait()
            few_ref[...] += erecv[src]
            remote(send.at[src], recv.at[src], ps.at[src], pr.at[src], k, beside).wait_send()

        @pl.when(jnp.logical_and(k != src, k + src != 3) if src in (0, 3) else k != src)
        def _():
            remote(send.at[src], recv.at[src], ps.at[src], pr.at[src], k, beside).wait_recv()

            def add(c, carry):
                at_rows = pl.ds(c * 16, 16)
                acc[at_rows, :] = acc[at_rows, :] + recv[src, at_rows, :].astype(f32)
                return carry

            lax.fori_loop(0, rows // 16, add, 0)


def project(x, gain, weights, forgetting, strength, state, keys, values, thin):
    rows, depth = x.shape
    width = weights[0].shape[1]
    vmem, hbm = pl.BlockSpec(memory_space=pltpu.VMEM), pl.BlockSpec(memory_space=pl.ANY)
    dma = pltpu.SemaphoreType.DMA
    heads = state.shape[1]
    return pl.pallas_call(
        project_kernel,
        in_specs=[vmem] * 5 + [hbm] * 7,
        out_specs=[vmem, vmem, hbm],
        out_shape=[
            jax.ShapeDtypeStruct((rows, 4 * width), f32),
            jax.ShapeDtypeStruct((40, rows), f32),
            jax.ShapeDtypeStruct(state.shape, f32),
        ],
        scratch_shapes=[
            pltpu.VMEM((4, rows, depth), bf16),
            pltpu.VMEM((4, depth, width), bf16),
            pltpu.VMEM((2, forgetting.shape[1], depth), bf16),
            pltpu.VMEM((4, rows, 4 * width), bf16),
            pltpu.VMEM((5, rows, 4 * width), bf16),
            pltpu.VMEM((4, 40, rows), f32),
            pltpu.VMEM((4, 40, rows), f32),
            pltpu.VMEM((2, SB) + state.shape[1:], f32),
            pltpu.VMEM((2, SB) + state.shape[1:], f32),
            *[pltpu.VMEM((heads * n, DK), f32) for n in (TALL, TALL, SB, TALL, TALL)],
            dma((4,)), dma((4,)), dma((6,)), dma((4,)), dma((5,)), dma((4,)), dma((4,)), dma((2,)), dma((2,)),
        ],
        compiler_params=pltpu.CompilerParams(has_side_effects=True, vmem_limit_bytes=56 * 2**20),
        name="project",
    )(x, gain.reshape(-1, 1, depth), keys, values, thin, *weights, forgetting.T, strength.T, state)


NEAREST = ((0, 1, 2, 3), (1, 0, 2, 3), (2, 3, 1, 0), (3, 2, 1, 0))


def mix_kernel(flat_ref, wo, o_ref, held, w, part, mate, cross, total, wsem, gs, gr, ms, mr, xs, xr, ts, tr):
    k, t, g = lax.axis_index("kv"), lax.axis_index("tp"), lax.axis_index("grp")
    rows = flat_ref.shape[0]

    def remote(src, dst, ss, rs, kv, tp):
        return pltpu.make_async_remote_copy(
            src, dst, ss, rs, device_id={"grp": g, "kv": kv, "tp": tp}, device_id_type=pl.DeviceIdType.MESH
        )

    load = pltpu.make_async_copy(wo, w, wsem.at[0])
    own = pltpu.make_async_copy(flat_ref, held.at[k], wsem.at[1])
    own.start()
    sends = [remote(flat_ref, held.at[k], gs.at[n], gr.at[k], lax.rem(k + n, 4), t) for n in (1, 2, 3)]
    for copy in sends:
        copy.start()
    load.start()
    beside = t + 1 - 2 * (t % 2)
    across = (t + 2) % 4
    diagonal = (beside + 2) % 4
    load.wait()
    own.wait()

    def to_mate(r, n):
        return remote(part.at[r], mate.at[n], ms.at[n], mr.at[n], k, beside)

    def to_cross(r):
        return remote(part.at[r], cross, xs, xr, k, across)

    def step(i, carry):
        r = pick(k, [pick(i, row) for row in NEAREST])

        @pl.when(r != k)
        def _():
            remote(held.at[r], held.at[r], gs.at[0], gr.at[r], r, t).wait_recv()

        part[r] = jnp.dot(held[r], w[...], preferred_element_type=f32).astype(bf16)
        sink = turned_slot(r)

        @pl.when(sink == beside)
        def _():
            to_mate(r, 0).start()

        @pl.when(sink == diagonal)
        def _():
            to_mate(r, 1).start()

        @pl.when(sink == across)
        def _():
            to_mate(r, 1).wait_recv()

            def add(c, carry):
                at_rows = pl.ds(c * 16, 16)
                part[r, at_rows, :] = (part[r, at_rows, :].astype(f32) + mate[1, at_rows, :].astype(f32)).astype(bf16)
                return carry

            lax.fori_loop(0, rows // 16, add, 0)
            to_cross(r).start()

        return carry

    lax.fori_loop(0, 4, step, 0)
    mine = turned_slot(t)
    to_mate(mine, 0).wait_recv()
    to_cross(mine).wait_recv()

    def add(c, carry):
        at_rows = pl.ds(c * 16, 16)
        total[at_rows, :] = (
            part[mine, at_rows, :].astype(f32) + mate[0, at_rows, :].astype(f32) + cross[at_rows, :].astype(f32)
        ).astype(bf16)
        return carry

    lax.fori_loop(0, rows // 16, add, 0)
    home = jnp.logical_and(mine == k, t == k)
    last = remote(total, o_ref, ts, tr, mine, k)
    local = pltpu.make_async_copy(total, o_ref, tr)

    @pl.when(home)
    def _():
        local.start()
        local.wait()

    @pl.when(jnp.logical_not(home))
    def _():
        last.start()
        last.wait()

    for copy in sends:
        copy.wait_send()
    to_mate(0, 0).wait_send()
    to_mate(0, 1).wait_send()
    to_cross(0).wait_send()


def mix(flat, final):
    rows, width = flat.shape
    cols = final.shape[1]
    vmem, hbm = pl.BlockSpec(memory_space=pltpu.VMEM), pl.BlockSpec(memory_space=pl.ANY)
    dma = pltpu.SemaphoreType.DMA
    return pl.pallas_call(
        mix_kernel,
        in_specs=[vmem, hbm],
        out_specs=vmem,
        out_shape=jax.ShapeDtypeStruct((rows, cols), bf16),
        scratch_shapes=[
            pltpu.VMEM((4, rows, width), bf16),
            pltpu.VMEM((width, cols), bf16),
            pltpu.VMEM((4, rows, cols), bf16),
            pltpu.VMEM((2, rows, cols), bf16),
            pltpu.VMEM((rows, cols), bf16),
            pltpu.VMEM((rows, cols), bf16),
            dma((2,)), dma((4,)), dma((4,)), dma((2,)), dma((2,)), dma, dma, dma, dma,
        ],
        compiler_params=pltpu.CompilerParams(has_side_effects=True, vmem_limit_bytes=56 * 2**20),
        name="mix",
    )(flat, final)


def on_device(
    n_kv,
    n_tp,
    candidate_embeddings,
    incoming_rms_scaling,
    probe_projector,
    address_projector,
    content_projector,
    sigmoid_mask_matrix,
    forgetting_projector,
    strength_projector_matrix,
    channel_forgetting_rates,
    forgetting_offset,
    extra_forgetting,
    outgoing_rms_scaling,
    final_projector,
    memory_matrix,
    earlier_addresses,
    earlier_contents,
    earlier_strengths,
    earlier_forgetting,
    admitted_counts,
):
    rows, local_cols = candidate_embeddings.shape
    features = incoming_rms_scaling.shape[0]
    depth, width = probe_projector.shape
    heads = width // DK
    seqs = rows // P_SIZE
    k_index, t_index = lax.axis_index("kv"), lax.axis_index("tp")

    def thin(values):
        return values.reshape(seqs, P_SIZE * heads)

    weights = (probe_projector, address_projector, content_projector, sigmoid_mask_matrix)
    earlier = (
        memory_matrix,
        earlier_addresses.reshape(rows, width),
        earlier_contents.reshape(rows, width),
        jnp.concatenate(
            [thin(earlier_forgetting), thin(earlier_strengths), admitted_counts.astype(f32).reshape(seqs, 1)], axis=1
        ),
    )
    if n_kv == 4 and n_tp == 4:
        summed, few, taken = project(
            candidate_embeddings, incoming_rms_scaling, weights, forgetting_projector, strength_projector_matrix, *earlier
        )
        columns = forgetting_projector.shape[1]
        few = [lax.dynamic_slice_in_dim(few, n * columns + t_index * heads, heads) for n in range(2)] + [few[2 * columns : 2 * columns + 1]]
        few = jnp.concatenate(few, axis=0).T
    else:
        every = lax.all_gather(candidate_embeddings, "tp", axis=1, tiled=True)
        every = lax.all_to_all(every, "kv", split_axis=1, concat_axis=0, tiled=True)
        gain_part = lax.dynamic_slice_in_dim(incoming_rms_scaling, k_index * depth, depth)
        floated = every.astype(f32)
        gained = (floated * gain_part).astype(bf16)
        decay_cols = lax.dynamic_slice(forgetting_projector, (k_index * depth, t_index * heads), (depth, heads))
        beta_cols = lax.dynamic_slice(strength_projector_matrix, (k_index * depth, t_index * heads), (depth, heads))
        few = jnp.concatenate(
            [
                jnp.dot(gained, jnp.concatenate([decay_cols, beta_cols], axis=1), preferred_element_type=f32),
                jnp.sum(floated * floated, axis=1, keepdims=True),
            ],
            axis=1,
        )
        few = lax.psum_scatter(few, "kv", scatter_dimension=0, tiled=True)
        partial = jnp.concatenate(
            [jnp.dot(gained, w, preferred_element_type=f32).astype(bf16) for w in weights], axis=1
        )
        summed = lax.psum_scatter(partial, "kv", scatter_dimension=0, tiled=True).astype(f32)
        taken = accepted(*earlier)
    factor = lax.rsqrt(few[:, 2 * heads :] / features + epsilon)
    few = few[:, : 2 * heads] * factor
    decay_in = few[:, :heads].reshape(seqs, P_SIZE, heads)
    beta = jax.nn.sigmoid(few[:, heads:].reshape(seqs, P_SIZE, heads))
    decay = -jnp.exp(channel_forgetting_rates) * jax.nn.softplus(decay_in + forgetting_offset) + extra_forgetting
    flat, taken = attend(taken, summed, factor, thin(decay), thin(beta), outgoing_rms_scaling)
    if n_kv == 4 and n_tp == 4:
        mixed = mix(flat, final_projector)
    else:
        gathered = lax.all_gather(flat, "kv", axis=0, tiled=True)
        terms = jnp.dot(gathered, final_projector, preferred_element_type=f32).astype(bf16)
        terms = lax.all_to_all(terms, "kv", split_axis=0, concat_axis=1, tiled=True)
        mixed = lax.psum_scatter(terms, "tp", scatter_dimension=1, tiled=True)
    return (mixed, taken)


def solution(mesh):
    row, per_head = P(("grp", "kv"), "tp"), P(("grp", "kv"), None, "tp")
    four = P(("grp", "kv"), None, "tp", None)
    weight = P("kv", "tp")
    state = P(("grp", "kv"), "tp", None, None)
    in_specs = (
        row, P(), weight, weight, weight, weight, P(), P(), P("tp"), P("tp"), per_head, P(),
        P("tp", "kv"), state, four, four, per_head, per_head, P(("grp", "kv")),
    )
    body = functools.partial(on_device, mesh.shape["kv"], mesh.shape["tp"])
    return jax.shard_map(body, mesh=mesh, in_specs=in_specs, out_specs=(row, state), check_vma=False)
```

profile of v0, /device:TPU:9, one launch (start us, length us, event | category | flops | bytes accessed | tf_op | source)
XLA Modules:
  0.0 167.0 jit_solution(3372160389569808868)
XLA Ops:
  0.6 0.0 copy-start
  0.6 0.0 copy-start.1
  0.7 0.7 exponential_negate_fusion
  1.3 0.7 convert_bitcast_fusion
  2.0 0.1 copy.45
  2.1 0.8 copy.44
  2.9 0.8 copy.43
  3.6 0.7 pad_maximum_fusion.thin
  4.3 1.8 %copy_bitcast_fusion = (bf16[192,512]{1,0:T(8,128)(2,1)}, bf16[192,512]{1,0:T(8,128)(2,1)}) fusion(bf16[24,8,4,128]{3,2,1,0:T(4,128)(2,1)} %bitcast.22, bf16[24,8,4,128]{3,2,1,0:T(4,128)(2,1)} %bitcast.23), kind=kLoop, calls=%fused_computation | loop fusion | bytes 786432 | tf_op jit(solution)/shard_map/reshape | solution.py:561
  6.1 88.1 %project.1 = (f32[192,2048]{1,0:T(8,128)}, f32[40,192]{1,0:T(8,128)}, f32[48,4,128,128]{3,2,1,0:T(8,128)}) custom-call(bf16[192,1024]{1,0:T(8,128)(2,1)} %x_ref.1, f32[4,1,1024]{2,1,0:T(1,128)} %bitcast.27, bf16[192,512]{1,0:T(8,128)(2,1)} %get-tuple-element.19.keys, bf16[192,512]{1,0:T(8,128)(2,1)} %get-tuple-element.18.values, ...), custom_call_target="tpu_custom_call" | custom-call | tf_op jit(solution)/shard_map/project/pallas_call | solution.py:376
  94.2 0.7 slice.15
  94.9 0.7 constant_dynamic-slice_fusion.1
  95.6 0.1 copy.46
  95.8 0.7 fusion.7
  96.5 0.1 slice_multiply_fusion
  96.6 0.1 fusion.2
  96.7 0.7 div.16.b_ref
  97.4 0.1 copy.47
  97.5 0.0 copy-done
  97.5 0.0 copy-done.1
  97.5 0.1 fusion.6
  97.6 0.7 copy.50.d_ref
  98.3 14.3 %attend.1 = (bf16[192,512]{1,0:T(8,128)(2,1)}, f32[48,4,128,128]{3,2,1,0:T(8,128)}) custom-call(f32[48,4,128,128]{3,2,1,0:T(8,128)} %get-tuple-element.7.s_ref, f32[192,1]{1,0:T(8,128)} %get-tuple-element.15.a_ref, f32[192,2048]{1,0:T(8,128)} %get-tuple-element.9.q_ref.k_ref.v_ref.z_ref, f32[192,2048]{1,0:T(8,128)} %get-tuple-element.9.q_ref.k_ref.v_ref.z_ref, ...), custom_call_target="tpu_custom_call" | custom-call | flops 5000000000 | bytes 12582912 | tf_op jit(solution)/shard_map/attend/pallas_call | solution.py:167
  112.5 52.7 %mix.1 = bf16[192,1024]{1,0:T(8,128)(2,1)} custom-call(bf16[192,512]{1,0:T(8,128)(2,1)} %get-tuple-element.10.flat_ref, bf16[512,1024]{1,0:T(8,128)(2,1)} %wo.1), custom_call_target="tpu_custom_call" | custom-call | tf_op jit(solution)/shard_map/mix/pallas_call | solution.py:505
  165.3 1.8 %copy.56 = bf16[192,1024]{1,0:T(8,128)(2,1)} copy(bf16[192,1024]{1,0:T(8,128)(2,1)} %mix.1) | data formatting | bytes 786432
  (1 shorter events, 0.0 us)
Async XLA Ops:
  0.6 96.9 %copy-start = (f32[48,4,4]{0,2,1:T(4,128)S(1)}, f32[48,4,4]{0,2,1:T(4,128)}, u32[]{:S(2)}) copy-start(f32[48,4,4]{0,2,1:T(4,128)} %param.29) | copy-start | bytes 9220
  0.6 96.9 %copy-start.1 = (f32[4]{0:T(128)S(1)}, f32[4]{0:T(128)}, u32[]{:S(2)}) copy-start(f32[4]{0:T(128)} %param.28) | copy-start | bytes 52
where the time goes:
time: 169 us; the launch traced here: 167 us
  Pallas kernels  155 us (92%)
  local copies, waits for them, and re-layouts  8.22 us (5%)
  other arithmetic  3.04 us (2%)
    pallas_call x1, Pallas kernels, project(): pl.pallas_call(project_kernel, in_specs=[vmem] * 5 + [hbm] * 7, out_specs...  88.1 us
    pallas_call x1, Pallas kernels, mix(): pl.pallas_call(mix_kernel, in_specs=[vmem, hbm], out_specs=vmem, out_shap...  52.7 us
    pallas_call x1, Pallas kernels, attend(): pl.pallas_call(functools.partial(attend_kernel, heads), grid=(seqs // SB,...  14.3 us

commit v1 on v0

--- a/solution.py
+++ b/solution.py
@@ -162,7 +162,7 @@
     block = pl.BlockSpec((SB, heads, DK, DK), lambda i: (i, 0, 0, 0))
 
     def part(n):
-        return pl.BlockSpec((rows, width), lambda i: (i, n))
+        return pl.BlockSpec((None, rows, width), lambda i: (n, i, 0))
 
     return pl.pallas_call(
         functools.partial(attend_kernel, heads),
@@ -187,25 +187,19 @@
     return pick(t, (0, 2, 1, 3))
 
 
-ORDER = ((3, 2, 1, 0), (0, 2, 1, 3), (3, 1, 2, 0), (0, 1, 2, 3))
-
-
-def project_kernel(x_ref, gain_ref, keys, values, thin, wq, wk, wv, wz, wf, ws, state, acc, few_ref, taken, xbuf, w, fs,
-                   send, recv, esend, erecv, s_in, s_out, r_scr, u_scr, c_scr, kf, vf,
-                   xs, xr, wsem, ps, pr, es, er, ins, outs):
+def project_kernel(x_ref, gain_ref, keys, values, thin, fs, wq, wk, wv, wz, wo, state, acc, few_ref, taken, f_out,
+                   xbuf, gbuf, w, fbuf, sbuf, abuf, bbuf, cbuf, esend, erecv, s_in, s_out, r_scr, u_scr, c_scr, kf, vf,
+                   xs, xr, wsem, ss, ar, br, cr, es, er, ins, outs, fsem, fss, fzr, fys, fyr, fos):
     k, t, g = lax.axis_index("kv"), lax.axis_index("tp"), lax.axis_index("grp")
     depth, width = w.shape[1], w.shape[2]
     rows = x_ref.shape[0]
 
-    def at(kv, tp):
-        return {"grp": g, "kv": kv, "tp": tp}
-
-    def remote(src, dst, ss, rs, kv, tp):
-        return pltpu.make_async_remote_copy(src, dst, ss, rs, device_id=at(kv, tp), device_id_type=pl.DeviceIdType.MESH)
+    def remote(src, dst, send, recv, kv, tp, grp=g):
+        return pltpu.make_async_remote_copy(
+            src, dst, send, recv, device_id={"grp": grp, "kv": kv, "tp": tp}, device_id_type=pl.DeviceIdType.MESH
+        )
 
     loads = [pltpu.make_async_copy(src, w.at[i], wsem.at[i]) for i, src in enumerate((wq, wk, wv, wz))]
-    here = pl.ds(k * depth, depth)
-    loads += [pltpu.make_async_copy(src.at[:, here], fs.at[i], wsem.at[4 + i]) for i, src in enumerate((wf, ws))]
     slot = turned_slot(t)
     far_t, far_k = turned_slot(k), t
     home = jnp.logical_and(far_k == k, far_t == t)
@@ -220,9 +214,22 @@
     def _():
         local.start()
 
+    f_load = pltpu.make_async_copy(wo, fbuf.at[k], fsem)
+    f_load.start()
     for load in loads:
         load.start()
 
+    blocks = state.shape[0] // SB
+    heads = state.shape[1]
+
+    def fetch(i):
+        return pltpu.make_async_copy(state.at[pl.ds(i * SB, SB)], s_in.at[i % 2], ins.at[i % 2])
+
+    def put(i):
+        return pltpu.make_async_copy(s_out.at[i % 2], taken.at[pl.ds(i * SB, SB)], outs.at[i % 2])
+
+    fetch(0).start()
+
     beside = t + 1 - 2 * (t % 2)
     across = (t + 2) % 4
 
@@ -239,8 +246,47 @@
 
     over = remote(xbuf.at[slot], xbuf.at[slot], xs.at[1], xr.at[slot], k, across)
     over.start()
-    near = remote(xbuf.at[slot], xbuf.at[slot], xs.at[2], xr.at[slot], k, beside)
-    near.start()
+    near_x = remote(xbuf.at[slot], xbuf.at[slot], xs.at[2], xr.at[slot], k, beside)
+    near_x.start()
+
+    half_rows = fbuf.shape[1] // 2
+    half = pl.ds(g * half_rows, half_rows)
+
+    def f_pass(c, to, sem):
+        return remote(fbuf.at[c, half], fbuf.at[c, half], fss.at[sem], fzr.at[c], to, t)
+
+    def f_swap(c):
+        return remote(fbuf.at[c, half], fbuf.at[c, half], fys.at[c], fyr.at[c], k, t, 1 - g)
+
+    f_load.wait()
+
+    @pl.when(k < 3)
+    def _():
+        f_pass(k, k + 1, 4).start()
+
+    @pl.when(k > 0)
+    def _():
+        f_pass(k, k - 1, 5).start()
+
+    def f_forwards(c):
+        return jnp.logical_or(jnp.logical_and(c < k, k < 3), jnp.logical_and(c > k, k > 0))
+
+    def f_take(c):
+        to = jnp.where(c < k, k + 1, k - 1)
+        f_pass(c, k, c).wait_recv()
+
+        @pl.when(f_forwards(c))
+        def _():
+            f_pass(c, to, c).start()
+
+        f_swap(c).start()
+
+    end = jnp.where(k <= 1, 0, 3)
+    near = jnp.where(k <= 1, 1, 2)
+    is_end = k == end
+    inside = jnp.logical_not(is_end)
+    f_order = (jnp.where(is_end, near, end), 3 - near, 3 - end)
+
     other = turned_slot(across)
     arrived(other)
     onward = remote(xbuf.at[other], xbuf.at[other], xs.at[3], xr.at[other], k, beside)
@@ -250,68 +296,38 @@
     for load in loads:
         load.wait()
 
-    def step(i, carry):
-        r = pick(k, [pick(i, row) for row in ORDER])
-        own = r == k
+    nt = (((1,), (1,)), ((), ()))
+    thin_rows = fs.shape[0]
+
+    def prepare(r):
         floated = xbuf[r].astype(f32)
         gained = (floated * gain_ref[k]).astype(bf16)
+        gbuf[r] = gained
         squares = floated * floated
         high = squares.astype(bf16)
         rest = (squares - high.astype(f32)).astype(bf16)
         ones = jnp.ones((8, depth), bf16)
-        nt = (((1,), (1,)), ((), ()))
-        esend[r, 0:16, :] = lax.dot_general(fs[0], gained, nt, preferred_element_type=f32)
-        esend[r, 16:32, :] = lax.dot_general(fs[1], gained, nt, preferred_element_type=f32)
-        esend[r, 32:40, :] = lax.dot_general(ones, high, nt, preferred_element_type=f32) + lax.dot_general(
+        esend[r, 0:thin_rows, :] = lax.dot_general(fs[...], gained, nt, preferred_element_type=f32)
+        esend[r, thin_rows:, :] = lax.dot_general(ones, high, nt, preferred_element_type=f32) + lax.dot_general(
             ones, rest, nt, preferred_element_type=f32
         )
-        for j in range(4):
-            part = jnp.dot(gained, w[j], preferred_element_type=f32)
-            cols = slice(j * width, (j + 1) * width)
-
-            @pl.when(own)
-            def _():
-                acc[:, cols] = part
-
-            @pl.when(jnp.logical_not(own))
-            def _():
-                send[r, :, cols] = part.astype(bf16)
-
-        relayed = jnp.logical_or(jnp.logical_and(k == 1, r == 3), jnp.logical_and(k == 2, r == 0))
-
-        @pl.when(relayed)
-        def _():
-            remote(send.at[r], recv.at[4], ps.at[r], pr.at[4], k, beside).wait_recv()
-
-            def add(c, carry):
-                at_rows = pl.ds(c * 16, 16)
-                send[r, at_rows, :] = (send[r, at_rows, :].astype(f32) + recv[4, at_rows, :].astype(f32)).astype(bf16)
-                return carry
-
-            lax.fori_loop(0, rows // 16, add, 0)
-
-        @pl.when(jnp.logical_not(own))
-        def _():
-            ends = jnp.logical_or(jnp.logical_and(k == 0, r == 3), jnp.logical_and(k == 3, r == 0))
-            target = jnp.where(ends, jnp.where(k == 0, 1, 2), r)
-            place = jnp.where(ends, 4, k)
-            remote(send.at[r], recv.at[place], ps.at[r], pr.at[place], target, t).start()
+
+        @pl.when(r != k)
+        def _():
             remote(esend.at[r], erecv.at[k], es.at[r], er.at[k], r, t).start()
 
-        return carry
-
-    lax.fori_loop(0, 3, step, 0)
-
-    blocks = state.shape[0] // SB
-    heads = state.shape[1]
-
-    def fetch(i):
-        return pltpu.make_async_copy(state.at[pl.ds(i * SB, SB)], s_in.at[i % 2], ins.at[i % 2])
-
-    def put(i):
-        return pltpu.make_async_copy(s_out.at[i % 2], taken.at[pl.ds(i * SB, SB)], outs.at[i % 2])
-
-    def accept(i, carry):
+    def product(r, c):
+        return jnp.dot(gbuf[r], w[c], preferred_element_type=f32)
+
+    def from_end(i):
+        remote(abuf.at[i], abuf.at[i], ss.at[i], ar.at[i], k, beside).wait_recv()
+        return abuf[i].astype(f32)
+
+    def from_inner(i):
+        remote(bbuf.at[i], bbuf.at[i], ss.at[i], br.at[i], k, beside).wait_recv()
+        return bbuf[i].astype(f32)
+
+    def accept(i):
         @pl.when(i + 1 < blocks)
         def _():
             fetch(i + 1).start()
@@ -328,23 +344,75 @@
             r_scr, u_scr, c_scr, kf, vf,
         )
         put(i).start()
+
+    def step(i, carry):
+        stage, c = i // 4, i % 4
+        r = pick(stage, (3 - end, 3 - near, near))
+
+        @pl.when(c == 0)
+        def _():
+            prepare(r)
+
+        @pl.when(i == 2)
+        def _():
+            prepare(end)
+
+        @pl.when(is_end)
+        def _():
+            sbuf[i] = product(r, c).astype(bf16)
+            remote(sbuf.at[i], abuf.at[i], ss.at[i], ar.at[i], near, t).start()
+
+        @pl.when(jnp.logical_and(inside, i == 1))
+        def _():
+            f_take(f_order[0])
+            f_take(f_order[1])
+
+        @pl.when(jnp.logical_and(inside, i == 5))
+        def _():
+            f_take(f_order[2])
+
+        @pl.when(jnp.logical_and(is_end, i == 4))
+        def _():
+            f_take(f_order[0])
+
+        @pl.when(jnp.logical_and(inside, i < 8))
+        def _():
+            part = product(r, c)
+            sbuf[i] = (part + from_end(i)).astype(bf16)
+            remote(sbuf.at[i], bbuf.at[i], ss.at[i], br.at[i], 3 - near, t).start()
+
+        @pl.when(jnp.logical_and(inside, stage == 1))
+        def _():
+            part = product(end, c)
+            sbuf[8 + c] = (part + from_inner(c)).astype(bf16)
+            remote(sbuf.at[8 + c], cbuf.at[c], ss.at[8 + c], cr.at[c], end, t).start()
+
+        @pl.when(jnp.logical_and(inside, stage == 2))
+        def _():
+            acc[c] = product(r, c) + from_inner(4 + c) + from_end(i)
+
+        @pl.when(i % 2 == 0)
+        def _():
+            accept(i // 2)
+
         return carry
 
-    fetch(0).start()
-    lax.fori_loop(0, blocks, accept, 0)
-    lax.fori_loop(3, 4, step, 0)
+    lax.fori_loop(0, 12, step, 0)
     for i in range(max(blocks - 2, 0), blocks):
         put(i).wait()
 
-    first_wait = jnp.logical_not(home)
-
-    @pl.when(first_wait)
-    def _():
-        first.wait_send()
-
-    over.wait_send()
-    near.wait_send()
-    onward.wait_send()
+    @pl.when(is_end)
+    def _():
+        f_take(f_order[1])
+
+        def finish(c, carry):
+            part = product(end, c)
+            remote(cbuf.at[c], cbuf.at[c], ss.at[c], cr.at[c], k, beside).wait_recv()
+            acc[c] = part + cbuf[c].astype(f32)
+            return carry
+
+        lax.fori_loop(0, 4, finish, 0)
+        f_take(f_order[2])
 
     few_ref[...] = esend[k]
     for src in range(4):
@@ -353,153 +421,144 @@
         def _():
             remote(esend.at[src], erecv.at[src], es.at[src], er.at[src], k, beside).wait()
             few_ref[...] += erecv[src]
-            remote(send.at[src], recv.at[src], ps.at[src], pr.at[src], k, beside).wait_send()
-
-        @pl.when(jnp.logical_and(k != src, k + src != 3) if src in (0, 3) else k != src)
-        def _():
-            remote(send.at[src], recv.at[src], ps.at[src], pr.at[src], k, beside).wait_recv()
-
-            def add(c, carry):
-                at_rows = pl.ds(c * 16, 16)
-                acc[at_rows, :] = acc[at_rows, :] + recv[src, at_rows, :].astype(f32)
-                return carry
-
-            lax.fori_loop(0, rows // 16, add, 0)
-
-
-def project(x, gain, weights, forgetting, strength, state, keys, values, thin):
+            remote(fbuf.at[src, half], fbuf.at[src, half], fys.at[src], fyr.at[src], k, beside).wait()
+
+        pltpu.make_async_copy(fbuf.at[src], f_out.at[src], fos.at[src]).start()
+
+    @pl.when(jnp.logical_not(home))
+    def _():
+        first.wait_send()
+
+    over.wait_send()
+    near_x.wait_send()
+    onward.wait_send()
+
+    @pl.when(k < 3)
+    def _():
+        f_pass(k, k, 4).wait_send()
+
+    @pl.when(k > 0)
+    def _():
+        f_pass(k, k, 5).wait_send()
+
+    for src in range(4):
+
+        @pl.when(jnp.logical_and(k != src, f_forwards(src)))
+        def _():
+            f_pass(src, k, src).wait_send()
+
+        pltpu.make_async_copy(fbuf.at[src], f_out.at[src], fos.at[src]).wait()
+
+    for i in range(12):
+        remote(sbuf.at[i], abuf.at[i], ss.at[i], ar.at[i], k, beside).wait_send()
+
+
+def project(x, gain, weights, few_weights, final, state, keys, values, thin):
     rows, depth = x.shape
     width = weights[0].shape[1]
+    thin_rows = few_weights.shape[0]
     vmem, hbm = pl.BlockSpec(memory_space=pltpu.VMEM), pl.BlockSpec(memory_space=pl.ANY)
     dma = pltpu.SemaphoreType.DMA
     heads = state.shape[1]
+
+    def chunks(n):
+        return pltpu.VMEM((n, rows, width), bf16)
+
     return pl.pallas_call(
         project_kernel,
-        in_specs=[vmem] * 5 + [hbm] * 7,
-        out_specs=[vmem, vmem, hbm],
+        in_specs=[vmem] * 6 + [hbm] * 6,
+        out_specs=[vmem, vmem, hbm, hbm],
         out_shape=[
-            jax.ShapeDtypeStruct((rows, 4 * width), f32),
-            jax.ShapeDtypeStruct((40, rows), f32),
+            jax.ShapeDtypeStruct((4, rows, width), f32),
+            jax.ShapeDtypeStruct((thin_rows + 8, rows), f32),
             jax.ShapeDtypeStruct(state.shape, f32),
+            jax.ShapeDtypeStruct((4,) + final.shape, bf16),
         ],
         scratch_shapes=[
             pltpu.VMEM((4, rows, depth), bf16),
+            pltpu.VMEM((4, rows, depth), bf16),
             pltpu.VMEM((4, depth, width), bf16),
-            pltpu.VMEM((2, forgetting.shape[1], depth), bf16),
-            pltpu.VMEM((4, rows, 4 * width), bf16),
-            pltpu.VMEM((5, rows, 4 * width), bf16),
-            pltpu.VMEM((4, 40, rows), f32),
-            pltpu.VMEM((4, 40, rows), f32),
+            pltpu.VMEM((4,) + final.shape, bf16),
+            chunks(12), chunks(12), chunks(8), chunks(4),
+            pltpu.VMEM((4, thin_rows + 8, rows), f32),
+            pltpu.VMEM((4, thin_rows + 8, rows), f32),
             pltpu.VMEM((2, SB) + state.shape[1:], f32),
             pltpu.VMEM((2, SB) + state.shape[1:], f32),
             *[pltpu.VMEM((heads * n, DK), f32) for n in (TALL, TALL, SB, TALL, TALL)],
-            dma((4,)), dma((4,)), dma((6,)), dma((4,)), dma((5,)), dma((4,)), dma((4,)), dma((2,)), dma((2,)),
+            dma((4,)), dma((4,)), dma((4,)), dma((12,)), dma((12,)), dma((8,)), dma((4,)), dma((4,)), dma((4,)),
+            dma((2,)), dma((2,)), dma, dma((6,)), dma((4,)), dma((4,)), dma((4,)), dma((4,)),
         ],
         compiler_params=pltpu.CompilerParams(has_side_effects=True, vmem_limit_bytes=56 * 2**20),
         name="project",
-    )(x, gain.reshape(-1, 1, depth), keys, values, thin, *weights, forgetting.T, strength.T, state)
-
-
-NEAREST = ((0, 1, 2, 3), (1, 0, 2, 3), (2, 3, 1, 0), (3, 2, 1, 0))
-
-
-def mix_kernel(flat_ref, wo, o_ref, held, w, part, mate, cross, total, wsem, gs, gr, ms, mr, xs, xr, ts, tr):
+    )(x, gain.reshape(-1, 1, depth), keys, values, thin, few_weights, *weights, final, state)
+
+
+PIECES = 3
+
+
+def mix_kernel(flat_ref, f_hbm, o_ref, w, part, mate, cross, wsem, ms, mr, xs, xr):
     k, t, g = lax.axis_index("kv"), lax.axis_index("tp"), lax.axis_index("grp")
     rows = flat_ref.shape[0]
-
-    def remote(src, dst, ss, rs, kv, tp):
-        return pltpu.make_async_remote_copy(
-            src, dst, ss, rs, device_id={"grp": g, "kv": kv, "tp": tp}, device_id_type=pl.DeviceIdType.MESH
-        )
-
-    load = pltpu.make_async_copy(wo, w, wsem.at[0])
-    own = pltpu.make_async_copy(flat_ref, held.at[k], wsem.at[1])
-    own.start()
-    sends = [remote(flat_ref, held.at[k], gs.at[n], gr.at[k], lax.rem(k + n, 4), t) for n in (1, 2, 3)]
-    for copy in sends:
-        copy.start()
-    load.start()
+    piece = rows // PIECES
     beside = t + 1 - 2 * (t % 2)
     across = (t + 2) % 4
-    diagonal = (beside + 2) % 4
-    load.wait()
-    own.wait()
-
-    def to_mate(r, n):
-        return remote(part.at[r], mate.at[n], ms.at[n], mr.at[n], k, beside)
-
-    def to_cross(r):
-        return remote(part.at[r], cross, xs, xr, k, across)
-
-    def step(i, carry):
-        r = pick(k, [pick(i, row) for row in NEAREST])
-
-        @pl.when(r != k)
-        def _():
-            remote(held.at[r], held.at[r], gs.at[0], gr.at[r], r, t).wait_recv()
-
-        part[r] = jnp.dot(held[r], w[...], preferred_element_type=f32).astype(bf16)
-        sink = turned_slot(r)
-
-        @pl.when(sink == beside)
-        def _():
-            to_mate(r, 0).start()
-
-        @pl.when(sink == diagonal)
-        def _():
-            to_mate(r, 1).start()
-
-        @pl.when(sink == across)
-        def _():
-            to_mate(r, 1).wait_recv()
-
-            def add(c, carry):
-                at_rows = pl.ds(c * 16, 16)
-                part[r, at_rows, :] = (part[r, at_rows, :].astype(f32) + mate[1, at_rows, :].astype(f32)).astype(bf16)
-                return carry
-
-            lax.fori_loop(0, rows // 16, add, 0)
-            to_cross(r).start()
-
-        return carry
-
-    lax.fori_loop(0, 4, step, 0)
-    mine = turned_slot(t)
-    to_mate(mine, 0).wait_recv()
-    to_cross(mine).wait_recv()
-
-    def add(c, carry):
-        at_rows = pl.ds(c * 16, 16)
-        total[at_rows, :] = (
-            part[mine, at_rows, :].astype(f32) + mate[0, at_rows, :].astype(f32) + cross[at_rows, :].astype(f32)
+    order = ((beside + 2) % 4, across, beside, t)
+
+    def remote(src, dst, send, recv, tp):
+        return pltpu.make_async_remote_copy(
+            src, dst, send, recv, device_id={"grp": g, "kv": k, "tp": tp}, device_id_type=pl.DeviceIdType.MESH
+        )
+
+    loads = [pltpu.make_async_copy(f_hbm.at[c], w.at[n], wsem.at[n]) for n, c in enumerate(order)]
+    for load in loads:
+        load.start()
+
+    def to_mate(n, s):
+        at = pl.ds(s * piece, piece)
+        return remote(part.at[2 * n, at], mate.at[n, at], ms.at[n, s], mr.at[n, s], beside)
+
+    def to_cross(s):
+        at = pl.ds(s * piece, piece)
+        return remote(part.at[1, at], cross.at[at], xs.at[s], xr.at[s], across)
+
+    def fill(n, s):
+        at = pl.ds(s * piece, piece)
+        return jnp.dot(flat_ref[at, :], w[n], preferred_element_type=f32).astype(bf16)
+
+    loads[0].wait()
+    for s in range(PIECES):
+        part[0, s * piece : (s + 1) * piece, :] = fill(0, s)
+        to_mate(0, s).start()
+    loads[1].wait()
+    for s in range(PIECES):
+        at = slice(s * piece, (s + 1) * piece)
+        mine = fill(1, s).astype(f32)
+        to_mate(0, s).wait_recv()
+        part[1, at, :] = (mine + mate[0, at, :].astype(f32)).astype(bf16)
+        to_cross(s).start()
+    loads[2].wait()
+    for s in range(PIECES):
+        part[2, s * piece : (s + 1) * piece, :] = fill(2, s)
+        to_mate(1, s).start()
+    loads[3].wait()
+    for s in range(PIECES):
+        part[3, s * piece : (s + 1) * piece, :] = fill(3, s)
+    for s in range(PIECES):
+        at = slice(s * piece, (s + 1) * piece)
+        to_mate(1, s).wait_recv()
+        to_cross(s).wait_recv()
+        o_ref[at, :] = (
+            part[3, at, :].astype(f32) + mate[1, at, :].astype(f32) + cross[at, :].astype(f32)
         ).astype(bf16)
-        return carry
-
-    lax.fori_loop(0, rows // 16, add, 0)
-    home = jnp.logical_and(mine == k, t == k)
-    last = remote(total, o_ref, ts, tr, mine, k)
-    local = pltpu.make_async_copy(total, o_ref, tr)
-
-    @pl.when(home)
-    def _():
-        local.start()
-        local.wait()
-
-    @pl.when(jnp.logical_not(home))
-    def _():
-        last.start()
-        last.wait()
-
-    for copy in sends:
-        copy.wait_send()
-    to_mate(0, 0).wait_send()
-    to_mate(0, 1).wait_send()
-    to_cross(0).wait_send()
+    for s in range(PIECES):
+        to_mate(0, s).wait_send()
+        to_mate(1, s).wait_send()
+        to_cross(s).wait_send()
 
 
 def mix(flat, final):
     rows, width = flat.shape
-    cols = final.shape[1]
+    cols = final.shape[2]
     vmem, hbm = pl.BlockSpec(memory_space=pltpu.VMEM), pl.BlockSpec(memory_space=pl.ANY)
     dma = pltpu.SemaphoreType.DMA
     return pl.pallas_call(
@@ -508,13 +567,11 @@
         out_specs=vmem,
         out_shape=jax.ShapeDtypeStruct((rows, cols), bf16),
         scratch_shapes=[
-            pltpu.VMEM((4, rows, width), bf16),
-            pltpu.VMEM((width, cols), bf16),
+            pltpu.VMEM((4, width, cols), bf16),
             pltpu.VMEM((4, rows, cols), bf16),
             pltpu.VMEM((2, rows, cols), bf16),
             pltpu.VMEM((rows, cols), bf16),
-            pltpu.VMEM((rows, cols), bf16),
-            dma((2,)), dma((4,)), dma((4,)), dma((2,)), dma((2,)), dma, dma, dma, dma,
+            dma((4,)), dma((2, PIECES)), dma((2, PIECES)), dma((PIECES,)), dma((PIECES,)),
         ],
         compiler_params=pltpu.CompilerParams(has_side_effects=True, vmem_limit_bytes=56 * 2**20),
         name="mix",
@@ -564,12 +621,17 @@
         ),
     )
     if n_kv == 4 and n_tp == 4:
-        summed, few, taken = project(
-            candidate_embeddings, incoming_rms_scaling, weights, forgetting_projector, strength_projector_matrix, *earlier
+        few_weights = jnp.concatenate(
+            [
+                lax.dynamic_slice(m, (k_index * depth, t_index * heads), (depth, heads))
+                for m in (forgetting_projector, strength_projector_matrix)
+            ],
+            axis=1,
+        ).T
+        summed, few, taken, columns = project(
+            candidate_embeddings, incoming_rms_scaling, weights, few_weights, final_projector, *earlier
         )
-        columns = forgetting_projector.shape[1]
-        few = [lax.dynamic_slice_in_dim(few, n * columns + t_index * heads, heads) for n in range(2)] + [few[2 * columns : 2 * columns + 1]]
-        few = jnp.concatenate(few, axis=0).T
+        few = few[: 2 * heads + 1].T
     else:
         every = lax.all_gather(candidate_embeddings, "tp", axis=1, tiled=True)
         every = lax.all_to_all(every, "kv", split_axis=1, concat_axis=0, tiled=True)
@@ -586,10 +648,8 @@
             axis=1,
         )
         few = lax.psum_scatter(few, "kv", scatter_dimension=0, tiled=True)
-        partial = jnp.concatenate(
-            [jnp.dot(gained, w, preferred_element_type=f32).astype(bf16) for w in weights], axis=1
-        )
-        summed = lax.psum_scatter(partial, "kv", scatter_dimension=0, tiled=True).astype(f32)
+        partial = jnp.stack([jnp.dot(gained, w, preferred_element_type=f32).astype(bf16) for w in weights])
+        summed = lax.psum_scatter(partial, "kv", scatter_dimension=1, tiled=True).astype(f32)
         taken = accepted(*earlier)
     factor = lax.rsqrt(few[:, 2 * heads :] / features + epsilon)
     few = few[:, : 2 * heads] * factor
@@ -598,7 +658,7 @@
     decay = -jnp.exp(channel_forgetting_rates) * jax.nn.softplus(decay_in + forgetting_offset) + extra_forgetting
     flat, taken = attend(taken, summed, factor, thin(decay), thin(beta), outgoing_rms_scaling)
     if n_kv == 4 and n_tp == 4:
-        mixed = mix(flat, final_projector)
+        mixed = mix(flat, columns)
     else:
         gathered = lax.all_gather(flat, "kv", axis=0, tiled=True)
         terms = jnp.dot(gathered, final_projector, preferred_element_type=f32).astype(bf16)

time: 169 us -> 155 us (0.917)
  Pallas kernels: 155 us -> 139 us
    pallas_call x1, Pallas kernels: 52.7 us -> 31.4 us  [mix(): pl.pallas_call(mix_kernel, in_specs=[vmem, hbm], out_specs=vmem, out_shap...]
    pallas_call x1, Pallas kernels: 88.1 us -> 93.3 us  [project(): pl.pallas_call(project_kernel, in_specs=[vmem] * 6 + [hbm] * 6, out_specs...]
where the time goes in v1:
time: 155 us; the launch traced here: 153 us
  Pallas kernels  139 us (90%)
  local copies, waits for them, and re-layouts  9.1 us (6%)
  other arithmetic  3.67 us (2%)
    pallas_call x1, Pallas kernels, project(): pl.pallas_call(project_kernel, in_specs=[vmem] * 6 + [hbm] * 6, out_specs...  93.3 us
    pallas_call x1, Pallas kernels, mix(): pl.pallas_call(mix_kernel, in_specs=[vmem, hbm], out_specs=vmem, out_shap...  31.4 us
    pallas_call x1, Pallas kernels, attend(): pl.pallas_call(functools.partial(attend_kernel, heads), grid=(seqs // SB,...  14.3 us

profile of v1, /device:TPU:9, one launch (start us, length us, event | category | flops | bytes accessed | tf_op | source)
XLA Modules:
  0.0 152.5 jit_solution(12212586130606557791)
XLA Ops:
  0.6 0.0 copy-start
  0.6 0.0 copy-start.1
  0.7 0.7 exponential_negate_fusion
  1.3 0.7 convert_bitcast_fusion
  2.0 0.8 dynamic_slice.6
  2.8 0.8 dynamic_slice.7
  3.6 0.6 maximum_bitcast_fusion.fs
  4.2 0.1 copy.35
  4.3 0.8 copy.34
  5.1 0.8 copy.33
  5.8 0.7 pad_maximum_fusion.thin
  6.5 1.8 %copy_bitcast_fusion = (bf16[192,512]{1,0:T(8,128)(2,1)}, bf16[192,512]{1,0:T(8,128)(2,1)}) fusion(bf16[24,8,4,128]{3,2,1,0:T(4,128)(2,1)} %bitcast.23, bf16[24,8,4,128]{3,2,1,0:T(4,128)(2,1)} %bitcast.24), kind=kLoop, calls=%fused_computation | loop fusion | bytes 786432 | tf_op jit(solution)/shard_map/reshape | solution.py:618
  8.3 93.3 %project.1 = (f32[4,192,512]{2,1,0:T(8,128)}, f32[16,192]{1,0:T(8,128)}, f32[48,4,128,128]{3,2,1,0:T(8,128)}, bf16[4,512,1024]{2,1,0:T(8,128)(2,1)}) custom-call(bf16[192,1024]{1,0:T(8,128)(2,1)} %x_ref.1, f32[4,1,1024]{2,1,0:T(1,128)} %bitcast.26, bf16[192,512]{1,0:T(8,128)(2,1)} %get-tuple-element.19.keys, bf16[192,512]{1,0:T(8,128)(2,1)} %get-tuple-element.18.values, ...), custom_call_target="tpu_custom_call" | custom-call | tf_op jit(solution)/shard_map/project/pallas_call | solution.py:467
  101.7 0.8 copy.36
  102.5 0.7 fusion.7
  103.2 0.1 slice_multiply_fusion
  103.3 0.1 fusion.2
  103.4 0.7 div.16.b_ref
  104.1 0.1 copy.37
  104.2 0.0 copy-done
  104.2 0.0 copy-done.1
  104.2 0.1 fusion.6
  104.3 0.7 copy.40.d_ref
  105.0 14.3 %attend.1 = (bf16[192,512]{1,0:T(8,128)(2,1)}, f32[48,4,128,128]{3,2,1,0:T(8,128)}) custom-call(f32[48,4,128,128]{3,2,1,0:T(8,128)} %get-tuple-element.8.s_ref, f32[192,1]{1,0:T(8,128)} %get-tuple-element.17.a_ref, f32[4,192,512]{2,1,0:T(8,128)} %get-tuple-element.10.q_ref.k_ref.v_ref.z_ref, f32[4,192,512]{2,1,0:T(8,128)} %get-tuple-element.10.q_ref.k_ref.v_ref.z_ref, ...), custom_call_target="tpu_custom_call" | custom-call | flops 5000000000 | bytes 12582912 | tf_op jit(solution)/shard_map/attend/pallas_call | solution.py:167
  119.3 31.4 %mix.1 = bf16[192,1024]{1,0:T(8,128)(2,1)} custom-call(bf16[192,512]{1,0:T(8,128)(2,1)} %get-tuple-element.11.flat_ref, bf16[4,512,1024]{2,1,0:T(8,128)(2,1)} %get-tuple-element.12.f_hbm), custom_call_target="tpu_custom_call" | custom-call | tf_op jit(solution)/shard_map/mix/pallas_call | solution.py:564
  150.7 1.8 %copy.46 = bf16[192,1024]{1,0:T(8,128)(2,1)} copy(bf16[192,1024]{1,0:T(8,128)(2,1)} %mix.1) | data formatting | bytes 786432
Async XLA Ops:
  0.6 103.6 %copy-start = (f32[48,4,4]{0,2,1:T(4,128)S(1)}, f32[48,4,4]{0,2,1:T(4,128)}, u32[]{:S(2)}) copy-start(f32[48,4,4]{0,2,1:T(4,128)} %param.29) | copy-start | bytes 9220
  0.6 103.6 %copy-start.1 = (f32[4]{0:T(128)S(1)}, f32[4]{0:T(128)}, u32[]{:S(2)}) copy-start(f32[4]{0:T(128)} %param.28) | copy-start | bytes 52

commit v2 on v1

--- a/solution.py
+++ b/solution.py
@@ -36,6 +36,15 @@
 
 def proposal(h, p):
     return pl.ds(h * TALL + p, SB, stride=P_SIZE)
+
+
+def rows_to_columns(wide):
+    count = wide.shape[1]
+    same = lax.broadcasted_iota(jnp.int32, (count, count), 0) == lax.broadcasted_iota(jnp.int32, (count, count), 1)
+    return lax.dot_general(
+        same.astype(f32), wide, (((1,), (1,)), ((), ())),
+        precision=lax.Precision.HIGHEST, preferred_element_type=f32,
+    )
 
 
 def accepted_kernel(heads, s_ref, k_ref, v_ref, n_ref, o_ref, r_scr, u_scr, c_scr, kf, vf):
@@ -90,49 +99,89 @@
                 o_ref[seq, h] = c_scr[pl.ds(h * SB + seq, 1), :] * s_ref[seq, h] + add
 
 
-def attend_kernel(heads, s_ref, a_ref, q_ref, k_ref, v_ref, z_ref, d_ref, b_ref, w_ref, o_ref, kept, rk, rq, qf, kf, vf, zf, of, done):
-    keep = pltpu.make_async_copy(s_ref, kept.at[pl.ds(pl.program_id(0) * SB, SB)], done)
-    keep.start()
-    for src, dst in ((q_ref, qf), (k_ref, kf), (v_ref, vf), (z_ref, zf)):
-        load_heads(heads, src, dst, a_ref[...])
+def attend_kernel(heads, features, few_ref, extra_ref, rate_ref, offset_ref, w_ref, parts_hbm, state, o_ref, kept,
+                  held, parts, thin, rk, rq, qf, kf, vf, zf, of, ins, outs, psem):
+    rows = o_ref.shape[0]
+    blocks = state.shape[0] // SB
+    pull = pltpu.make_async_copy(parts_hbm, parts, psem)
+    pull.start()
+
+    def fetch(i):
+        return pltpu.make_async_copy(state.at[pl.ds(i * SB, SB)], held.at[pl.ds(i * SB, SB)], ins.at[i])
+
+    def put(i):
+        return pltpu.make_async_copy(held.at[pl.ds(i * SB, SB)], kept.at[pl.ds(i * SB, SB)], outs.at[i])
+
+    for i in range(blocks):
+        fetch(i).start()
+    few = rows_to_columns(few_ref[...])
+    factor = lax.rsqrt(few[:, 2 * heads : 2 * heads + 1] / features + epsilon)
+    seqs = extra_ref.shape[1]
+    row = lax.broadcasted_iota(jnp.int32, (rows, seqs), 0)
+    owner = jnp.right_shift(row, 2) == lax.broadcasted_iota(jnp.int32, (rows, seqs), 1)
+    spread = lax.dot_general(
+        owner.astype(f32), extra_ref[...], (((1,), (1,)), ((), ())),
+        precision=lax.Precision.HIGHEST, preferred_element_type=f32,
+    )
+    turn = jnp.bitwise_and(lax.broadcasted_iota(jnp.int32, (rows, heads), 0), 3)
+    extra = pick(turn, [spread[:, p * heads : (p + 1) * heads] for p in range(P_SIZE)])
+    raised = few[:, :heads] * factor + offset_ref[...]
+    soft = jnp.maximum(raised, 0.0) + jnp.log1p(jnp.exp(-jnp.abs(raised)))
+    thin[:, :heads] = jnp.exp(extra - jnp.exp(rate_ref[...]) * soft)
+    thin[:, heads : 2 * heads] = jax.nn.sigmoid(few[:, heads : 2 * heads] * factor)
+    thin[:, 2 * heads : 2 * heads + 1] = factor
+    pull.wait()
     low = first_half()
-    for pair in range(SB // 2):
+    gain = w_ref[...]
+
+    def block(i, carry):
+        base = i * TALL
+        tall = pl.ds(base, TALL)
+        fetch(i).wait()
+        put(i).start()
+        scaling = thin[tall, 2 * heads : 2 * heads + 1]
+        for n, dst in enumerate((qf, kf, vf, zf)):
+            load_heads(heads, parts.at[n, tall], dst, scaling)
+        for pair in range(SB // 2):
+            for h in range(heads):
+                at = tile(h, pair)
+                lhs = jnp.concatenate([kf[at, :], qf[at, :]], axis=0).astype(bf16)
+                r0 = jnp.dot(lhs, held[i * SB + 2 * pair, h].astype(bf16), preferred_element_type=f32)
+                r1 = jnp.dot(lhs, held[i * SB + 2 * pair + 1, h].astype(bf16), preferred_element_type=f32)
+                rk[at, :] = jnp.where(low, r0[:8], r1[:8])
+                rq[at, :] = jnp.where(low, r0[8:], r1[8:])
         for h in range(heads):
-            at = tile(h, pair)
-            lhs = jnp.concatenate([kf[at, :], qf[at, :]], axis=0).astype(bf16)
-            r0 = jnp.dot(lhs, s_ref[2 * pair, h].astype(bf16), preferred_element_type=f32)
-            r1 = jnp.dot(lhs, s_ref[2 * pair + 1, h].astype(bf16), preferred_element_type=f32)
-            rk[at, :] = jnp.where(low, r0[:8], r1[:8])
-            rq[at, :] = jnp.where(low, r0[8:], r1[8:])
-    gain = w_ref[...]
-    for h in range(heads):
-        scale = jnp.ones((SB, 1), f32)
-        ks, us, norms = [], [], []
-        for p in range(P_SIZE):
-            at = proposal(h, p)
-            col = slice(p * heads + h, p * heads + h + 1)
-            key = kf[at, :]
-            query = qf[at, :]
-            norm = lax.rsqrt(lane_dot(key, key) + epsilon)
-            qnorm = lax.rsqrt(lane_dot(query, query) + epsilon) * DK ** (-0.5)
-            g = jnp.exp(d_ref[:, col])
-            rec = (scale * norm) * rk[at, :]
-            for ki, ui, ni in zip(ks, us, norms):
-                rec = rec + (lane_dot(ki, key) * (ni * norm)) * ui
-            us = [ui * g for ui in us]
-            scale = scale * g
-            us.append(b_ref[:, col] * (vf[at, :] - g * rec))
-            ks.append(key)
-            norms.append(norm)
-            att = (scale * qnorm) * rq[at, :]
-            for ki, ui, ni in zip(ks, us, norms):
-                att = att + (lane_dot(ki, query) * (ni * qnorm)) * ui
-            gate = zf[at, :]
-            mean = jnp.sum(att * att, axis=-1, keepdims=True) / DK
-            of[at, :] = att * lax.rsqrt(mean + epsilon) * gain * (gate * jax.nn.sigmoid(gate))
-    for h in range(heads):
-        o_ref[:, h * DK : (h + 1) * DK] = of[pl.ds(h * TALL, TALL), :].astype(bf16)
-    keep.wait()
+            scale = jnp.ones((SB, 1), f32)
+            ks, us, norms = [], [], []
+            for p in range(P_SIZE):
+                at = proposal(h, p)
+                scalars = thin[pl.ds(base + p, SB, stride=P_SIZE), :]
+                key = kf[at, :]
+                query = qf[at, :]
+                norm = lax.rsqrt(lane_dot(key, key) + epsilon)
+                qnorm = lax.rsqrt(lane_dot(query, query) + epsilon) * DK ** (-0.5)
+                g = scalars[:, h : h + 1]
+                rec = (scale * norm) * rk[at, :]
+                for ki, ui, ni in zip(ks, us, norms):
+                    rec = rec + (lane_dot(ki, key) * (ni * norm)) * ui
+                us = [ui * g for ui in us]
+                scale = scale * g
+                us.append(scalars[:, heads + h : heads + h + 1] * (vf[at, :] - g * rec))
+                ks.append(key)
+                norms.append(norm)
+                att = (scale * qnorm) * rq[at, :]
+                for ki, ui, ni in zip(ks, us, norms):
+                    att = att + (lane_dot(ki, query) * (ni * qnorm)) * ui
+                gate = zf[at, :]
+                mean = jnp.sum(att * att, axis=-1, keepdims=True) / DK
+                of[at, :] = att * lax.rsqrt(mean + epsilon) * gain * (gate * jax.nn.sigmoid(gate))
+        for h in range(heads):
+            o_ref[tall, h * DK : (h + 1) * DK] = of[pl.ds(h * TALL, TALL), :].astype(bf16)
+        return carry
+
+    lax.fori_loop(0, blocks, block, 0)
+    for i in range(blocks):
+        put(i).wait()
 
 
 def accepted(state, keys, values, few):
@@ -154,26 +203,28 @@
     )(state, keys, values, few)
 
 
-def attend(state, packed, factor, decay, beta, gain):
+def attend(features, state, parts, few, extra, rates, offset, gain):
     seqs, heads = state.shape[:2]
-    width = heads * DK
-    rows = TALL
-    thin = pl.BlockSpec((SB, P_SIZE * heads), lambda i: (i, 0))
-    block = pl.BlockSpec((SB, heads, DK, DK), lambda i: (i, 0, 0, 0))
-
-    def part(n):
-        return pl.BlockSpec((None, rows, width), lambda i: (n, i, 0))
-
+    rows, width = parts.shape[1:]
+    blocks = seqs // SB
+    vmem, hbm = pl.BlockSpec(memory_space=pltpu.VMEM), pl.BlockSpec(memory_space=pl.ANY)
+    dma = pltpu.SemaphoreType.DMA
     return pl.pallas_call(
-        functools.partial(attend_kernel, heads),
-        grid=(seqs // SB,),
-        in_specs=[block, pl.BlockSpec((rows, 1), lambda i: (i, 0)), part(0), part(1), part(2), part(3), thin, thin, pl.BlockSpec((1, DK), lambda i: (0, 0))],
-        out_specs=[pl.BlockSpec((rows, width), lambda i: (i, 0)), pl.BlockSpec(memory_space=pl.ANY)],
-        out_shape=[jax.ShapeDtypeStruct((seqs * P_SIZE, width), bf16), jax.ShapeDtypeStruct(state.shape, f32)],
-        scratch_shapes=[pltpu.VMEM((heads * TALL, DK), f32)] * 7 + [pltpu.SemaphoreType.DMA],
+        functools.partial(attend_kernel, heads, features),
+        in_specs=[vmem] * 5 + [hbm] * 2,
+        out_specs=[vmem, hbm],
+        out_shape=[jax.ShapeDtypeStruct((rows, width), bf16), jax.ShapeDtypeStruct(state.shape, f32)],
+        scratch_shapes=[
+            pltpu.VMEM(state.shape, f32),
+            pltpu.VMEM(parts.shape, f32),
+            pltpu.VMEM((rows, 2 * heads + 8), f32),
+            *[pltpu.VMEM((heads * TALL, DK), f32)] * 7,
+            dma((blocks,)), dma((blocks,)), dma,
+        ],
+        compiler_params=pltpu.CompilerParams(vmem_limit_bytes=40 * 2**20),
         cost_estimate=pl.CostEstimate(flops=5_000_000_000, bytes_accessed=state.size * 4, transcendentals=0),
         name="attend",
-    )(state, factor, packed, packed, packed, packed, decay, beta, gain.reshape(1, DK))
+    )(few, extra, rates.reshape(1, heads), offset.reshape(1, heads), gain.reshape(1, DK), parts, state)
 
 
 def pick(index, values):
@@ -187,41 +238,41 @@
     return pick(t, (0, 2, 1, 3))
 
 
-def project_kernel(x_ref, gain_ref, keys, values, thin, fs, wq, wk, wv, wz, wo, state, acc, few_ref, taken, f_out,
-                   xbuf, gbuf, w, fbuf, sbuf, abuf, bbuf, cbuf, esend, erecv, s_in, s_out, r_scr, u_scr, c_scr, kf, vf,
-                   xs, xr, wsem, ss, ar, br, cr, es, er, ins, outs, fsem, fss, fzr, fys, fyr, fos):
+def project_kernel(x_hbm, gain_hbm, keys_hbm, values_hbm, fade_hbm, pull_hbm, count_hbm, wf, ws, wq, wk, wv, wz, wo,
+                   state, acc_out, few_ref, taken, f_out,
+                   x_ref, gain_ref, keys, values, fade, pull, counts, fs, thin,
+                   xpre, xbuf, gbuf, w, fbuf, acc, sbuf, abuf, bbuf, cbuf, esend, erecv, s_in, s_out,
+                   r_scr, u_scr, c_scr, kf, vf,
+                   lsem, xs, xp, xr, wsem, ss, ar, br, cr, es, er, ins, outs, fsem, fss, fzr, fys, fyr, fos, aos):
     k, t, g = lax.axis_index("kv"), lax.axis_index("tp"), lax.axis_index("grp")
     depth, width = w.shape[1], w.shape[2]
     rows = x_ref.shape[0]
+    blocks = state.shape[0] // SB
+    heads = state.shape[1]
 
     def remote(src, dst, send, recv, kv, tp, grp=g):
         return pltpu.make_async_remote_copy(
             src, dst, send, recv, device_id={"grp": grp, "kv": kv, "tp": tp}, device_id_type=pl.DeviceIdType.MESH
         )
 
-    loads = [pltpu.make_async_copy(src, w.at[i], wsem.at[i]) for i, src in enumerate((wq, wk, wv, wz))]
-    slot = turned_slot(t)
-    far_t, far_k = turned_slot(k), t
-    home = jnp.logical_and(far_k == k, far_t == t)
-    first = remote(x_ref, xbuf.at[k], xs.at[0], xr.at[k], far_k, far_t)
-    local = pltpu.make_async_copy(x_ref, xbuf.at[k], xr.at[k])
-
-    @pl.when(jnp.logical_not(home))
-    def _():
-        first.start()
-
-    @pl.when(home)
-    def _():
-        local.start()
-
+    here = pl.ds(k * depth, depth)
+    locals_ = [
+        pltpu.make_async_copy(src, dst, lsem.at[n])
+        for n, (src, dst) in enumerate(
+            (
+                (x_hbm, x_ref), (gain_hbm, gain_ref), (keys_hbm, keys), (values_hbm, values), (fade_hbm, fade),
+                (pull_hbm, pull), (count_hbm, counts), (wf.at[:, here], fs.at[0]), (ws.at[:, here], fs.at[1]),
+            )
+        )
+    ]
+    for load in locals_:
+        load.start()
     f_load = pltpu.make_async_copy(wo, fbuf.at[k], fsem)
     f_load.start()
+    loads = [pltpu.make_async_copy(src, w.at[i], wsem.at[i]) for i, src in enumerate((wq, wk, wv, wz))]
     for load in loads:
         load.start()
 
-    blocks = state.shape[0] // SB
-    heads = state.shape[1]
-
     def fetch(i):
         return pltpu.make_async_copy(state.at[pl.ds(i * SB, SB)], s_in.at[i % 2], ins.at[i % 2])
 
@@ -232,22 +283,89 @@
 
     beside = t + 1 - 2 * (t % 2)
     across = (t + 2) % 4
-
-    def arrived(s):
-        remote(xbuf.at[s], xbuf.at[s], xs.at[0], xr.at[s], k, beside).wait_recv()
+    corner = t % 2
+    landing = 2 * (t // 2) + k % 2
+    home = corner == k % 2
+    top_kind = t // 2 == k // 2
+    source = jnp.where(top_kind, k, (k + 2) % 4)
+    near_src = jnp.where(k <= 1, corner, corner + 2)
+    far_src = jnp.where(k <= 1, corner + 2, corner)
+    barrier = pltpu.get_barrier_semaphore()
+
+    def greet(kv, tp, grp=g):
+        pl.semaphore_signal(
+            barrier, inc=1, device_id={"grp": grp, "kv": kv, "tp": tp}, device_id_type=pl.DeviceIdType.MESH
+        )
+
+    greet(k, beside)
+    greet(k, across)
+    greet(k, t, 1 - g)
+    for step in range(1, 4):
+        greet((k + step) % 4, t)
+
+    @pl.when(t != k)
+    def _():
+        greet(t, landing)
+
+    @pl.when(across != k)
+    def _():
+        greet(across, landing)
+
+    @pl.when(near_src != k)
+    def _():
+        greet(near_src, source)
+
+    @pl.when(far_src != k)
+    def _():
+        greet(far_src, source)
 
     @pl.when(home)
     def _():
-        local.wait()
+        pl.semaphore_wait(barrier, 8)
 
     @pl.when(jnp.logical_not(home))
     def _():
-        arrived(slot)
-
-    over = remote(xbuf.at[slot], xbuf.at[slot], xs.at[1], xr.at[slot], k, across)
-    over.start()
-    near_x = remote(xbuf.at[slot], xbuf.at[slot], xs.at[2], xr.at[slot], k, beside)
-    near_x.start()
+        pl.semaphore_wait(barrier, 10)
+
+    half_tall = rows // 2
+    top, bottom = pl.ds(0, half_tall), pl.ds(half_tall, half_tall)
+    locals_[0].wait()
+
+    @pl.when(t == k)
+    def _():
+        remote(x_ref.at[bottom], xbuf.at[k, bottom], xs.at[0], xr.at[k, 1], k, across).start()
+        pltpu.make_async_copy(x_ref.at[top], xbuf.at[k, top], xr.at[k, 0]).start()
+
+    @pl.when(t != k)
+    def _():
+        remote(x_ref.at[bottom], xpre, xs.at[0], xp, k, across).start()
+        remote(x_ref.at[top], xbuf.at[k, top], xs.at[1], xr.at[k, 0], t, landing).start()
+
+    @pl.when(across != k)
+    def _():
+        remote(xpre, xpre, xs.at[0], xp, k, across).wait_recv()
+        remote(xpre, xbuf.at[k, bottom], xs.at[2], xr.at[k, 1], across, landing).start()
+
+    kind = jnp.where(top_kind, 0, 1)
+    direct = pl.ds(kind * half_tall, half_tall)
+    crossed = pl.ds((1 - kind) * half_tall, half_tall)
+
+    def piece(r, at, send, kd, tp):
+        return remote(xbuf.at[r, at], xbuf.at[r, at], xs.at[send], xr.at[r, kd], k, tp)
+
+    def spread(r, n):
+        settled = jnp.logical_and(t == k, r == k)
+
+        @pl.when(settled)
+        def _():
+            pltpu.make_async_copy(x_ref.at[top], xbuf.at[k, top], xr.at[k, 0]).wait()
+
+        @pl.when(jnp.logical_not(settled))
+        def _():
+            piece(r, direct, 3, kind, across).wait_recv()
+
+        piece(r, direct, 3 + n, kind, across).start()
+        piece(r, direct, 5 + n, kind, beside).start()
 
     half_rows = fbuf.shape[1] // 2
     half = pl.ds(g * half_rows, half_rows)
@@ -258,6 +376,7 @@
     def f_swap(c):
         return remote(fbuf.at[c, half], fbuf.at[c, half], fys.at[c], fyr.at[c], k, t, 1 - g)
 
+    spread(near_src, 0)
     f_load.wait()
 
     @pl.when(k < 3)
@@ -267,6 +386,11 @@
     @pl.when(k > 0)
     def _():
         f_pass(k, k - 1, 5).start()
+
+    spread(far_src, 1)
+    for n, r in enumerate((near_src, far_src)):
+        piece(r, crossed, 3, 1 - kind, across).wait_recv()
+        piece(r, crossed, 7 + n, 1 - kind, beside).start()
 
     def f_forwards(c):
         return jnp.logical_or(jnp.logical_and(c < k, k < 3), jnp.logical_and(c > k, k > 0))
@@ -287,17 +411,18 @@
     inside = jnp.logical_not(is_end)
     f_order = (jnp.where(is_end, near, end), 3 - near, 3 - end)
 
-    other = turned_slot(across)
-    arrived(other)
-    onward = remote(xbuf.at[other], xbuf.at[other], xs.at[3], xr.at[other], k, beside)
-    onward.start()
-    arrived(turned_slot(beside))
-    arrived(turned_slot((beside + 2) % 4))
+    for load in locals_[1:]:
+        load.wait()
+    thin[...] = rows_to_columns(
+        jnp.concatenate([fade[...], pull[...], jnp.broadcast_to(counts[...].astype(f32), (8, counts.shape[1]))], axis=0)
+    )
     for load in loads:
         load.wait()
+    for r in (1 - corner, 3 - corner):
+        for kd in range(2):
+            piece(r, pl.ds(kd * half_tall, half_tall), 3, kd, beside).wait_recv()
 
     nt = (((1,), (1,)), ((), ()))
-    thin_rows = fs.shape[0]
 
     def prepare(r):
         floated = xbuf[r].astype(f32)
@@ -307,8 +432,10 @@
         high = squares.astype(bf16)
         rest = (squares - high.astype(f32)).astype(bf16)
         ones = jnp.ones((8, depth), bf16)
-        esend[r, 0:thin_rows, :] = lax.dot_general(fs[...], gained, nt, preferred_element_type=f32)
-        esend[r, thin_rows:, :] = lax.dot_general(ones, high, nt, preferred_element_type=f32) + lax.dot_general(
+        for n in range(2):
+            every = lax.dot_general(fs[n], gained, nt, preferred_element_type=f32)
+            esend[r, n * heads : (n + 1) * heads, :] = pick(t, [every[m * heads : (m + 1) * heads] for m in range(4)])
+        esend[r, 2 * heads :, :] = lax.dot_general(ones, high, nt, preferred_element_type=f32) + lax.dot_general(
             ones, rest, nt, preferred_element_type=f32
         )
 
@@ -390,6 +517,7 @@
         @pl.when(jnp.logical_and(inside, stage == 2))
         def _():
             acc[c] = product(r, c) + from_inner(4 + c) + from_end(i)
+            pltpu.make_async_copy(acc.at[c], acc_out.at[c], aos.at[c]).start()
 
         @pl.when(i % 2 == 0)
         def _():
@@ -407,12 +535,17 @@
 
         def finish(c, carry):
             part = product(end, c)
+
+            @pl.when(c == 1)
+            def _():
+                f_take(f_order[2])
+
             remote(cbuf.at[c], cbuf.at[c], ss.at[c], cr.at[c], k, beside).wait_recv()
             acc[c] = part + cbuf[c].astype(f32)
+            pltpu.make_async_copy(acc.at[c], acc_out.at[c], aos.at[c]).start()
             return carry
 
         lax.fori_loop(0, 4, finish, 0)
-        f_take(f_order[2])
 
     few_ref[...] = esend[k]
     for src in range(4):
@@ -425,13 +558,18 @@
 
         pltpu.make_async_copy(fbuf.at[src], f_out.at[src], fos.at[src]).start()
 
-    @pl.when(jnp.logical_not(home))
-    def _():
-        first.wait_send()
-
-    over.wait_send()
-    near_x.wait_send()
-    onward.wait_send()
+    remote(x_ref.at[bottom], xpre, xs.at[0], xp, k, across).wait_send()
+
+    @pl.when(t != k)
+    def _():
+        remote(x_ref.at[top], xbuf.at[k, top], xs.at[1], xr.at[k, 0], t, landing).wait_send()
+
+    @pl.when(across != k)
+    def _():
+        remote(xpre, xbuf.at[k, bottom], xs.at[2], xr.at[k, 1], across, landing).wait_send()
+
+    for n in range(6):
+        piece(k, top, 3 + n, 0, beside).wait_send()
 
     @pl.when(k < 3)
     def _():
@@ -446,51 +584,62 @@
         @pl.when(jnp.logical_and(k != src, f_forwards(src)))
         def _():
             f_pass(src, k, src).wait_send()
-
-        pltpu.make_async_copy(fbuf.at[src], f_out.at[src], fos.at[src]).wait()
 
     for i in range(12):
         remote(sbuf.at[i], abuf.at[i], ss.at[i], ar.at[i], k, beside).wait_send()
-
-
-def project(x, gain, weights, few_weights, final, state, keys, values, thin):
+    for src in range(4):
+        pltpu.make_async_copy(fbuf.at[src], f_out.at[src], fos.at[src]).wait()
+        pltpu.make_async_copy(acc.at[src], acc_out.at[src], aos.at[src]).wait()
+
+
+def project(x, gain, weights, forgetting, strength, final, state, keys, values, fade, pull, counts):
     rows, depth = x.shape
     width = weights[0].shape[1]
-    thin_rows = few_weights.shape[0]
+    seqs, heads = state.shape[:2]
+    few_rows = 2 * heads + 8
     vmem, hbm = pl.BlockSpec(memory_space=pltpu.VMEM), pl.BlockSpec(memory_space=pl.ANY)
     dma = pltpu.SemaphoreType.DMA
-    heads = state.shape[1]
+    gain = gain.reshape(-1, 1, depth)
+    forgetting, strength = forgetting.T, strength.T
 
     def chunks(n):
         return pltpu.VMEM((n, rows, width), bf16)
 
+    def like(a):
+        return pltpu.VMEM(a.shape, a.dtype)
+
     return pl.pallas_call(
         project_kernel,
-        in_specs=[vmem] * 6 + [hbm] * 6,
-        out_specs=[vmem, vmem, hbm, hbm],
+        in_specs=[hbm] * 15,
+        out_specs=[hbm, vmem, hbm, hbm],
         out_shape=[
             jax.ShapeDtypeStruct((4, rows, width), f32),
-            jax.ShapeDtypeStruct((thin_rows + 8, rows), f32),
+            jax.ShapeDtypeStruct((few_rows, rows), f32),
             jax.ShapeDtypeStruct(state.shape, f32),
             jax.ShapeDtypeStruct((4,) + final.shape, bf16),
         ],
         scratch_shapes=[
+            like(x), like(gain), like(keys), like(values), like(fade), like(pull), like(counts),
+            pltpu.VMEM((2, forgetting.shape[0], depth), bf16),
+            pltpu.VMEM((seqs, 2 * P_SIZE * heads + 8), f32),
+            pltpu.VMEM((rows // 2, depth), bf16),
             pltpu.VMEM((4, rows, depth), bf16),
             pltpu.VMEM((4, rows, depth), bf16),
             pltpu.VMEM((4, depth, width), bf16),
             pltpu.VMEM((4,) + final.shape, bf16),
+            pltpu.VMEM((4, rows, width), f32),
             chunks(12), chunks(12), chunks(8), chunks(4),
-            pltpu.VMEM((4, thin_rows + 8, rows), f32),
-            pltpu.VMEM((4, thin_rows + 8, rows), f32),
+            pltpu.VMEM((4, few_rows, rows), f32),
+            pltpu.VMEM((4, few_rows, rows), f32),
             pltpu.VMEM((2, SB) + state.shape[1:], f32),
             pltpu.VMEM((2, SB) + state.shape[1:], f32),
             *[pltpu.VMEM((heads * n, DK), f32) for n in (TALL, TALL, SB, TALL, TALL)],
-            dma((4,)), dma((4,)), dma((4,)), dma((12,)), dma((12,)), dma((8,)), dma((4,)), dma((4,)), dma((4,)),
-            dma((2,)), dma((2,)), dma, dma((6,)), dma((4,)), dma((4,)), dma((4,)), dma((4,)),
+            dma((9,)), dma((9,)), dma, dma((4, 2)), dma((4,)), dma((12,)), dma((12,)), dma((8,)), dma((4,)), dma((4,)),
+            dma((4,)), dma((2,)), dma((2,)), dma, dma((6,)), dma((4,)), dma((4,)), dma((4,)), dma((4,)), dma((4,)),
         ],
-        compiler_params=pltpu.CompilerParams(has_side_effects=True, vmem_limit_bytes=56 * 2**20),
+        compiler_params=pltpu.CompilerParams(has_side_effects=True, collective_id=0, vmem_limit_bytes=56 * 2**20),
         name="project",
-    )(x, gain.reshape(-1, 1, depth), keys, values, thin, few_weights, *weights, final, state)
+    )(x, gain, keys, values, fade, pull, counts, forgetting, strength, *weights, final, state)
 
 
 PIECES = 3
@@ -512,6 +661,12 @@
     loads = [pltpu.make_async_copy(f_hbm.at[c], w.at[n], wsem.at[n]) for n, c in enumerate(order)]
     for load in loads:
         load.start()
+    barrier = pltpu.get_barrier_semaphore()
+    for peer in (beside, across):
+        pl.semaphore_signal(
+            barrier, inc=1, device_id={"grp": g, "kv": k, "tp": peer}, device_id_type=pl.DeviceIdType.MESH
+        )
+    pl.semaphore_wait(barrier, 2)
 
     def to_mate(n, s):
         at = pl.ds(s * piece, piece)
@@ -573,7 +728,7 @@
             pltpu.VMEM((rows, cols), bf16),
             dma((4,)), dma((2, PIECES)), dma((2, PIECES)), dma((PIECES,)), dma((PIECES,)),
         ],
-        compiler_params=pltpu.CompilerParams(has_side_effects=True, vmem_limit_bytes=56 * 2**20),
+        compiler_params=pltpu.CompilerParams(has_side_effects=True, collective_id=1, vmem_limit_bytes=56 * 2**20),
         name="mix",
     )(flat, final)
 
@@ -609,29 +764,16 @@
     k_index, t_index = lax.axis_index("kv"), lax.axis_index("tp")
 
     def thin(values):
-        return values.reshape(seqs, P_SIZE * heads)
+        return values.transpose(1, 2, 0).reshape(P_SIZE * heads, seqs)
 
     weights = (probe_projector, address_projector, content_projector, sigmoid_mask_matrix)
-    earlier = (
-        memory_matrix,
-        earlier_addresses.reshape(rows, width),
-        earlier_contents.reshape(rows, width),
-        jnp.concatenate(
-            [thin(earlier_forgetting), thin(earlier_strengths), admitted_counts.astype(f32).reshape(seqs, 1)], axis=1
-        ),
-    )
+    fade, pull, extra = thin(earlier_forgetting), thin(earlier_strengths), thin(extra_forgetting)
+    earlier = (memory_matrix, earlier_addresses.reshape(rows, width), earlier_contents.reshape(rows, width))
     if n_kv == 4 and n_tp == 4:
-        few_weights = jnp.concatenate(
-            [
-                lax.dynamic_slice(m, (k_index * depth, t_index * heads), (depth, heads))
-                for m in (forgetting_projector, strength_projector_matrix)
-            ],
-            axis=1,
-        ).T
         summed, few, taken, columns = project(
-            candidate_embeddings, incoming_rms_scaling, weights, few_weights, final_projector, *earlier
+            candidate_embeddings, incoming_rms_scaling, weights, forgetting_projector, strength_projector_matrix,
+            final_projector, *earlier, fade, pull, admitted_counts.reshape(1, seqs),
         )
-        few = few[: 2 * heads + 1].T
     else:
         every = lax.all_gather(candidate_embeddings, "tp", axis=1, tiled=True)
         every = lax.all_to_all(every, "kv", split_axis=1, concat_axis=0, tiled=True)
@@ -648,15 +790,14 @@
             axis=1,
         )
         few = lax.psum_scatter(few, "kv", scatter_dimension=0, tiled=True)
+        few = jnp.pad(few, ((0, 0), (0, 7))).T
         partial = jnp.stack([jnp.dot(gained, w, preferred_element_type=f32).astype(bf16) for w in weights])
         summed = lax.psum_scatter(partial, "kv", scatter_dimension=1, tiled=True).astype(f32)
-        taken = accepted(*earlier)
-    factor = lax.rsqrt(few[:, 2 * heads :] / features + epsilon)
-    few = few[:, : 2 * heads] * factor
-    decay_in = few[:, :heads].reshape(seqs, P_SIZE, heads)
-    beta = jax.nn.sigmoid(few[:, heads:].reshape(seqs, P_SIZE, heads))
-    decay = -jnp.exp(channel_forgetting_rates) * jax.nn.softplus(decay_in + forgetting_offset) + extra_forgetting
-    flat, taken = attend(taken, summed, factor, thin(decay), thin(beta), outgoing_rms_scaling)
+        counts = admitted_counts.astype(f32).reshape(seqs, 1)
+        taken = accepted(*earlier, jnp.concatenate([fade.T, pull.T, counts], axis=1))
+    flat, taken = attend(
+        features, taken, summed, few, extra, channel_forgetting_rates, forgetting_offset, outgoing_rms_scaling
+    )
     if n_kv == 4 and n_tp == 4:
         mixed = mix(flat, columns)
     else:

time: 155 us -> 125 us (0.81)
  Pallas kernels: 139 us -> 111 us
  other arithmetic: 3.67 us -> 0 us
  local copies, waits for them, and re-layouts: 9.1 us -> 11 us
    pallas_call x1, Pallas kernels: 31.4 us -> 16.1 us  [mix(): pl.pallas_call(mix_kernel, in_specs=[vmem, hbm], out_specs=vmem, out_shap...]
    pallas_call x2, Pallas kernels: 108 us -> 94.7 us  [the longest x1 84.3 us: project(): pl.pallas_call(project_kernel, in_specs=[hbm] * 15, out_specs=[hbm, vmem,...]
    unnamed x5 -> x17, local copies, waits for them, and re-layouts: 1.78 us -> 9.15 us
    reshape x5 -> x0, local copies, waits for them, and re-layouts: 2.41 us -> none  [the longest x3 2.22 us: thin(): return values.reshape(seqs, P_SIZE * heads)]
    dynamic_slice x2 -> x0, local copies, waits for them, and re-layouts: 1.59 us -> none  [on_device(): lax.dynamic_slice(m, (k_index * depth, t_index * heads), (depth, heads))]
where the time goes in v2:
time: 125 us; the launch traced here: 122 us
  Pallas kernels  111 us (89%)
  local copies, waits for them, and re-layouts  11 us (9%)
    pallas_call x1, Pallas kernels, project(): pl.pallas_call(project_kernel, in_specs=[hbm] * 15, out_specs=[hbm, vmem,...  84.3 us
    pallas_call x1, Pallas kernels, mix(): pl.pallas_call(mix_kernel, in_specs=[vmem, hbm], out_specs=vmem, out_shap...  16.1 us
    pallas_call x1, Pallas kernels, attend(): pl.pallas_call(functools.partial(attend_kernel, heads, features), in_spec...  10.4 us
    unnamed x17, local copies, waits for them, and re-layouts  9.15 us

profile of v2, /device:TPU:9, one launch (start us, length us, event | category | flops | bytes accessed | tf_op | source)
XLA Modules:
  0.0 122.5 jit_solution(4585332090182929914)
XLA Ops:
  0.6 0.0 copy-start.7
  0.6 0.0 copy-start.4
  0.7 0.0 copy-start.6
  0.7 0.0 copy-start.5
  0.7 1.8 %copy_bitcast_fusion = (bf16[192,512]{1,0:T(8,128)(2,1)}, bf16[192,512]{1,0:T(8,128)(2,1)}) fusion(bf16[24,8,4,128]{3,2,1,0:T(4,128)(2,1)} %bitcast.28, bf16[24,8,4,128]{3,2,1,0:T(4,128)(2,1)} %bitcast.29), kind=kLoop, calls=%fused_computation | loop fusion | bytes 786432 | tf_op jit(solution)/shard_map/reshape | solution.py:771
  2.5 84.3 %project.1 = (f32[4,192,512]{2,1,0:T(8,128)}, f32[16,192]{1,0:T(8,128)}, f32[48,4,128,128]{3,2,1,0:T(8,128)}, bf16[4,512,1024]{2,1,0:T(8,128)(2,1)}) custom-call(bf16[192,1024]{1,0:T(8,128)(2,1)} %x_hbm.1, f32[4,1,1024]{2,1,0:T(1,128)} %bitcast.32, bf16[192,512]{1,0:T(8,128)(2,1)} %get-tuple-element.15.keys_hbm, ...), custom_call_target="tpu_custom_call" | custom-call | tf_op jit(solution)/shard_map/project/pallas_call | solution.py:611
  86.8 0.0 copy-done.7
  86.8 0.0 copy-done.4
  86.9 0.0 copy-done.6
  86.9 0.0 copy-done.5
  86.9 0.0 copy-start.1
  86.9 4.6 %copy-done.1 = f32[48,4,128,128]{3,2,1,0:T(8,128)S(1)} copy-done((f32[48,4,128,128]{3,2,1,0:T(8,128)S(1)}, f32[48,4,128,128]{3,2,1,0:T(8,128)}, u32[]{:S(2)}) %copy-start.1) | copy-done | bytes 12582936
  91.4 0.0 copy-start.2
  91.5 1.4 %copy-done.2 = f32[4,192,512]{2,1,0:T(8,128)S(1)} copy-done((f32[4,192,512]{2,1,0:T(8,128)S(1)}, f32[4,192,512]{2,1,0:T(8,128)}, u32[]{:S(2)}) %copy-start.2) | copy-done | bytes 1572888
  92.9 0.0 copy-start.3
  92.9 0.7 copy-done.3
  93.6 10.4 %attend.1 = (bf16[192,512]{1,0:T(8,128)(2,1)S(1)}, f32[48,4,128,128]{3,2,1,0:T(8,128)}) custom-call(f32[16,192]{1,0:T(8,128)S(1)} %copy-done.3, f32[16,48]{1,0:T(8,128)S(1)} %bitcast.24, f32[1,4]{1,0:T(1,128)S(1)} %bitcast.25, f32[1,4]{1,0:T(1,128)S(1)} %bitcast.26, f32[1,128]{1,0:T(1,128)S(1)} %bitcast.27, f32[4,192,512]{2,1,0:T(8,128)S(1)} %copy-done.2, ...), custom_call_target="tpu_custom_call" | custom-call | flops 5000000000 | bytes 12582912 | tf_op jit(solution)/shard_map/attend/pallas_call | solution.py:212
  104.0 0.0 copy-start
  104.0 0.7 copy-done
  104.6 16.1 %mix.1 = bf16[192,1024]{1,0:T(8,128)(2,1)} custom-call(bf16[192,512]{1,0:T(8,128)(2,1)} %copy-done, bf16[4,512,1024]{2,1,0:T(8,128)(2,1)} %get-tuple-element.12.f_hbm), custom_call_target="tpu_custom_call" | custom-call | tf_op jit(solution)/shard_map/mix/pallas_call | solution.py:719
  120.7 1.8 %copy.26 = bf16[192,1024]{1,0:T(8,128)(2,1)} copy(bf16[192,1024]{1,0:T(8,128)(2,1)} %mix.1) | data formatting | bytes 786432
Async XLA Ops:
  0.6 86.2 %copy-start.7 = (f32[128]{0:T(128)S(1)}, f32[128]{0:T(128)}, u32[]{:S(2)}) copy-start(f32[128]{0:T(128)} %param.30) | copy-start | bytes 1540
  0.6 86.2 %copy-start.4 = (f32[48,4,4]{0,2,1:T(4,128)S(1)}, f32[48,4,4]{0,2,1:T(4,128)}, u32[]{:S(2)}) copy-start(f32[48,4,4]{0,2,1:T(4,128)} %param.29) | copy-start | bytes 9220
  0.7 86.2 %copy-start.6 = (f32[4]{0:T(128)S(1)}, f32[4]{0:T(128)}, u32[]{:S(2)}) copy-start(f32[4]{0:T(128)} %param.28) | copy-start | bytes 52
  0.7 86.2 %copy-start.5 = (f32[4]{0:T(128)S(1)}, f32[4]{0:T(128)}, u32[]{:S(2)}) copy-start(f32[4]{0:T(128)} %param.27) | copy-start | bytes 52
  86.9 4.6 %copy-start.1 = (f32[48,4,128,128]{3,2,1,0:T(8,128)S(1)}, f32[48,4,128,128]{3,2,1,0:T(8,128)}, u32[]{:S(2)}) copy-start(f32[48,4,128,128]{3,2,1,0:T(8,128)} %get-tuple-element.10.state) | copy-start | bytes 37748740
  91.4 1.4 %copy-start.2 = (f32[4,192,512]{2,1,0:T(8,128)S(1)}, f32[4,192,512]{2,1,0:T(8,128)}, u32[]{:S(2)}) copy-start(f32[4,192,512]{2,1,0:T(8,128)} %get-tuple-element.9.parts_hbm) | copy-start | bytes 4718596
  92.9 0.7 copy-start.3
  104.0 0.7 copy-start

commit v3 on v2

--- a/solution.py
+++ b/solution.py
@@ -12,6 +12,7 @@
 SB = 8
 TALL = SB * P_SIZE
 epsilon = 1e-06
+LIMIT = 42 * 2**20
 f32 = jnp.float32
 bf16 = jnp.bfloat16
 
@@ -99,21 +100,11 @@
                 o_ref[seq, h] = c_scr[pl.ds(h * SB + seq, 1), :] * s_ref[seq, h] + add
 
 
-def attend_kernel(heads, features, few_ref, extra_ref, rate_ref, offset_ref, w_ref, parts_hbm, state, o_ref, kept,
-                  held, parts, thin, rk, rq, qf, kf, vf, zf, of, ins, outs, psem):
+def attend_kernel(heads, features, few_ref, extra_ref, rate_ref, offset_ref, w_ref, parts, state, o_ref, kept, thin, rk, rq, qf, kf, vf, zf, of, done):
+    keep = pltpu.make_async_copy(state, kept, done)
+    keep.start()
     rows = o_ref.shape[0]
     blocks = state.shape[0] // SB
-    pull = pltpu.make_async_copy(parts_hbm, parts, psem)
-    pull.start()
-
-    def fetch(i):
-        return pltpu.make_async_copy(state.at[pl.ds(i * SB, SB)], held.at[pl.ds(i * SB, SB)], ins.at[i])
-
-    def put(i):
-        return pltpu.make_async_copy(held.at[pl.ds(i * SB, SB)], kept.at[pl.ds(i * SB, SB)], outs.at[i])
-
-    for i in range(blocks):
-        fetch(i).start()
     few = rows_to_columns(few_ref[...])
     factor = lax.rsqrt(few[:, 2 * heads : 2 * heads + 1] / features + epsilon)
     seqs = extra_ref.shape[1]
@@ -130,15 +121,12 @@
     thin[:, :heads] = jnp.exp(extra - jnp.exp(rate_ref[...]) * soft)
     thin[:, heads : 2 * heads] = jax.nn.sigmoid(few[:, heads : 2 * heads] * factor)
     thin[:, 2 * heads : 2 * heads + 1] = factor
-    pull.wait()
     low = first_half()
     gain = w_ref[...]
 
     def block(i, carry):
         base = i * TALL
         tall = pl.ds(base, TALL)
-        fetch(i).wait()
-        put(i).start()
         scaling = thin[tall, 2 * heads : 2 * heads + 1]
         for n, dst in enumerate((qf, kf, vf, zf)):
             load_heads(heads, parts.at[n, tall], dst, scaling)
@@ -146,8 +134,8 @@
             for h in range(heads):
                 at = tile(h, pair)
                 lhs = jnp.concatenate([kf[at, :], qf[at, :]], axis=0).astype(bf16)
-                r0 = jnp.dot(lhs, held[i * SB + 2 * pair, h].astype(bf16), preferred_element_type=f32)
-                r1 = jnp.dot(lhs, held[i * SB + 2 * pair + 1, h].astype(bf16), preferred_element_type=f32)
+                r0 = jnp.dot(lhs, state[i * SB + 2 * pair, h].astype(bf16), preferred_element_type=f32)
+                r1 = jnp.dot(lhs, state[i * SB + 2 * pair + 1, h].astype(bf16), preferred_element_type=f32)
                 rk[at, :] = jnp.where(low, r0[:8], r1[:8])
                 rq[at, :] = jnp.where(low, r0[8:], r1[8:])
         for h in range(heads):
@@ -180,8 +168,7 @@
         return carry
 
     lax.fori_loop(0, blocks, block, 0)
-    for i in range(blocks):
-        put(i).wait()
+    keep.wait()
 
 
 def accepted(state, keys, values, few):
@@ -203,28 +190,31 @@
     )(state, keys, values, few)
 
 
+def local(array):
+    return pltpu.with_memory_space_constraint(array, pltpu.VMEM)
+
+
 def attend(features, state, parts, few, extra, rates, offset, gain):
     seqs, heads = state.shape[:2]
     rows, width = parts.shape[1:]
-    blocks = seqs // SB
-    vmem, hbm = pl.BlockSpec(memory_space=pltpu.VMEM), pl.BlockSpec(memory_space=pl.ANY)
-    dma = pltpu.SemaphoreType.DMA
+    vmem = pl.BlockSpec(memory_space=pltpu.VMEM)
     return pl.pallas_call(
         functools.partial(attend_kernel, heads, features),
-        in_specs=[vmem] * 5 + [hbm] * 2,
-        out_specs=[vmem, hbm],
-        out_shape=[jax.ShapeDtypeStruct((rows, width), bf16), jax.ShapeDtypeStruct(state.shape, f32)],
+        in_specs=[vmem] * 7,
+        out_specs=[vmem, pl.BlockSpec(memory_space=pl.ANY)],
+        out_shape=[pltpu.VMEM((rows, width), bf16), jax.ShapeDtypeStruct(state.shape, f32)],
         scratch_shapes=[
-            pltpu.VMEM(state.shape, f32),
-            pltpu.VMEM(parts.shape, f32),
             pltpu.VMEM((rows, 2 * heads + 8), f32),
             *[pltpu.VMEM((heads * TALL, DK), f32)] * 7,
-            dma((blocks,)), dma((blocks,)), dma,
+            pltpu.SemaphoreType.DMA,
         ],
-        compiler_params=pltpu.CompilerParams(vmem_limit_bytes=40 * 2**20),
+        compiler_params=pltpu.CompilerParams(vmem_limit_bytes=LIMIT),
         cost_estimate=pl.CostEstimate(flops=5_000_000_000, bytes_accessed=state.size * 4, transcendentals=0),
         name="attend",
-    )(few, extra, rates.reshape(1, heads), offset.reshape(1, heads), gain.reshape(1, DK), parts, state)
+    )(
+        local(few), extra, rates.reshape(1, heads), offset.reshape(1, heads), gain.reshape(1, DK),
+        local(parts), local(state),
+    )
 
 
 def pick(index, values):
@@ -239,11 +229,11 @@
 
 
 def project_kernel(x_hbm, gain_hbm, keys_hbm, values_hbm, fade_hbm, pull_hbm, count_hbm, wf, ws, wq, wk, wv, wz, wo,
-                   state, acc_out, few_ref, taken, f_out,
+                   state, acc, few_ref, taken, fbuf,
                    x_ref, gain_ref, keys, values, fade, pull, counts, fs, thin,
-                   xpre, xbuf, gbuf, w, fbuf, acc, sbuf, abuf, bbuf, cbuf, esend, erecv, s_in, s_out,
+                   xpre, xbuf, gbuf, w, sbuf, abuf, bbuf, cbuf, esend, erecv, s_in,
                    r_scr, u_scr, c_scr, kf, vf,
-                   lsem, xs, xp, xr, wsem, ss, ar, br, cr, es, er, ins, outs, fsem, fss, fzr, fys, fyr, fos, aos):
+                   lsem, xs, xp, xr, wsem, ss, ar, br, cr, es, er, ins, fsem, fss, fzr, fys, fyr):
     k, t, g = lax.axis_index("kv"), lax.axis_index("tp"), lax.axis_index("grp")
     depth, width = w.shape[1], w.shape[2]
     rows = x_ref.shape[0]
@@ -275,9 +265,6 @@
 
     def fetch(i):
         return pltpu.make_async_copy(state.at[pl.ds(i * SB, SB)], s_in.at[i % 2], ins.at[i % 2])
-
-    def put(i):
-        return pltpu.make_async_copy(s_out.at[i % 2], taken.at[pl.ds(i * SB, SB)], outs.at[i % 2])
 
     fetch(0).start()
 
@@ -377,6 +364,7 @@
         return remote(fbuf.at[c, half], fbuf.at[c, half], fys.at[c], fyr.at[c], k, t, 1 - g)
 
     spread(near_src, 0)
+    spread(far_src, 1)
     f_load.wait()
 
     @pl.when(k < 3)
@@ -387,7 +375,6 @@
     def _():
         f_pass(k, k - 1, 5).start()
 
-    spread(far_src, 1)
     for n, r in enumerate((near_src, far_src)):
         piece(r, crossed, 3, 1 - kind, across).wait_recv()
         piece(r, crossed, 7 + n, 1 - kind, beside).start()
@@ -461,16 +448,11 @@
 
         fetch(i).wait()
 
-        @pl.when(i >= 2)
-        def _():
-            put(i - 2).wait()
-
         tall, few_rows = pl.ds(i * TALL, TALL), pl.ds(i * SB, SB)
         accepted_kernel(
-            heads, s_in.at[i % 2], keys.at[tall], values.at[tall], thin.at[few_rows], s_out.at[i % 2],
+            heads, s_in.at[i % 2], keys.at[tall], values.at[tall], thin.at[few_rows], taken.at[few_rows],
             r_scr, u_scr, c_scr, kf, vf,
         )
-        put(i).start()
 
     def step(i, carry):
         stage, c = i // 4, i % 4
@@ -517,7 +499,6 @@
         @pl.when(jnp.logical_and(inside, stage == 2))
         def _():
             acc[c] = product(r, c) + from_inner(4 + c) + from_end(i)
-            pltpu.make_async_copy(acc.at[c], acc_out.at[c], aos.at[c]).start()
 
         @pl.when(i % 2 == 0)
         def _():
@@ -526,8 +507,6 @@
         return carry
 
     lax.fori_loop(0, 12, step, 0)
-    for i in range(max(blocks - 2, 0), blocks):
-        put(i).wait()
 
     @pl.when(is_end)
     def _():
@@ -542,7 +521,6 @@
 
             remote(cbuf.at[c], cbuf.at[c], ss.at[c], cr.at[c], k, beside).wait_recv()
             acc[c] = part + cbuf[c].astype(f32)
-            pltpu.make_async_copy(acc.at[c], acc_out.at[c], aos.at[c]).start()
             return carry
 
         lax.fori_loop(0, 4, finish, 0)
@@ -556,8 +534,6 @@
             few_ref[...] += erecv[src]
             remote(fbuf.at[src, half], fbuf.at[src, half], fys.at[src], fyr.at[src], k, beside).wait()
 
-        pltpu.make_async_copy(fbuf.at[src], f_out.at[src], fos.at[src]).start()
-
     remote(x_ref.at[bottom], xpre, xs.at[0], xp, k, across).wait_send()
 
     @pl.when(t != k)
@@ -587,9 +563,6 @@
 
     for i in range(12):
         remote(sbuf.at[i], abuf.at[i], ss.at[i], ar.at[i], k, beside).wait_send()
-    for src in range(4):
-        pltpu.make_async_copy(fbuf.at[src], f_out.at[src], fos.at[src]).wait()
-        pltpu.make_async_copy(acc.at[src], acc_out.at[src], aos.at[src]).wait()
 
 
 def project(x, gain, weights, forgetting, strength, final, state, keys, values, fade, pull, counts):
@@ -611,12 +584,12 @@
     return pl.pallas_call(
         project_kernel,
         in_specs=[hbm] * 15,
-        out_specs=[hbm, vmem, hbm, hbm],
+        out_specs=[vmem] * 4,
         out_shape=[
-            jax.ShapeDtypeStruct((4, rows, width), f32),
-            jax.ShapeDtypeStruct((few_rows, rows), f32),
-            jax.ShapeDtypeStruct(state.shape, f32),
-            jax.ShapeDtypeStruct((4,) + final.shape, bf16),
+            pltpu.VMEM((4, rows, width), f32),
+            pltpu.VMEM((few_rows, rows), f32),
+            pltpu.VMEM(state.shape, f32),
+            pltpu.VMEM((4,) + final.shape, bf16),
         ],
         scratch_shapes=[
             like(x), like(gain), like(keys), like(values), like(fade), like(pull), like(counts),
@@ -626,18 +599,15 @@
             pltpu.VMEM((4, rows, depth), bf16),
             pltpu.VMEM((4, rows, depth), bf16),
             pltpu.VMEM((4, depth, width), bf16),
-            pltpu.VMEM((4,) + final.shape, bf16),
-            pltpu.VMEM((4, rows, width), f32),
             chunks(12), chunks(12), chunks(8), chunks(4),
             pltpu.VMEM((4, few_rows, rows), f32),
             pltpu.VMEM((4, few_rows, rows), f32),
             pltpu.VMEM((2, SB) + state.shape[1:], f32),
-            pltpu.VMEM((2, SB) + state.shape[1:], f32),
             *[pltpu.VMEM((heads * n, DK), f32) for n in (TALL, TALL, SB, TALL, TALL)],
             dma((9,)), dma((9,)), dma, dma((4, 2)), dma((4,)), dma((12,)), dma((12,)), dma((8,)), dma((4,)), dma((4,)),
-            dma((4,)), dma((2,)), dma((2,)), dma, dma((6,)), dma((4,)), dma((4,)), dma((4,)), dma((4,)), dma((4,)),
+            dma((4,)), dma((2,)), dma, dma((6,)), dma((4,)), dma((4,)), dma((4,)),
         ],
-        compiler_params=pltpu.CompilerParams(has_side_effects=True, collective_id=0, vmem_limit_bytes=56 * 2**20),
+        compiler_params=pltpu.CompilerParams(has_side_effects=True, collective_id=0, vmem_limit_bytes=LIMIT),
         name="project",
     )(x, gain, keys, values, fade, pull, counts, forgetting, strength, *weights, final, state)
 
@@ -645,7 +615,7 @@
 PIECES = 3
 
 
-def mix_kernel(flat_ref, f_hbm, o_ref, w, part, mate, cross, wsem, ms, mr, xs, xr):
+def mix_kernel(flat_ref, f_ref, o_ref, part, mate, cross, ms, mr, xs, xr):
     k, t, g = lax.axis_index("kv"), lax.axis_index("tp"), lax.axis_index("grp")
     rows = flat_ref.shape[0]
     piece = rows // PIECES
@@ -658,9 +628,6 @@
             src, dst, send, recv, device_id={"grp": g, "kv": k, "tp": tp}, device_id_type=pl.DeviceIdType.MESH
         )
 
-    loads = [pltpu.make_async_copy(f_hbm.at[c], w.at[n], wsem.at[n]) for n, c in enumerate(order)]
-    for load in loads:
-        load.start()
     barrier = pltpu.get_barrier_semaphore()
     for peer in (beside, across):
         pl.semaphore_signal(
@@ -678,24 +645,20 @@
 
     def fill(n, s):
         at = pl.ds(s * piece, piece)
-        return jnp.dot(flat_ref[at, :], w[n], preferred_element_type=f32).astype(bf16)
-
-    loads[0].wait()
+        return jnp.dot(flat_ref[at, :], f_ref[order[n]], preferred_element_type=f32).astype(bf16)
+
     for s in range(PIECES):
         part[0, s * piece : (s + 1) * piece, :] = fill(0, s)
         to_mate(0, s).start()
-    loads[1].wait()
     for s in range(PIECES):
         at = slice(s * piece, (s + 1) * piece)
         mine = fill(1, s).astype(f32)
         to_mate(0, s).wait_recv()
         part[1, at, :] = (mine + mate[0, at, :].astype(f32)).astype(bf16)
         to_cross(s).start()
-    loads[2].wait()
     for s in range(PIECES):
         part[2, s * piece : (s + 1) * piece, :] = fill(2, s)
         to_mate(1, s).start()
-    loads[3].wait()
     for s in range(PIECES):
         part[3, s * piece : (s + 1) * piece, :] = fill(3, s)
     for s in range(PIECES):
@@ -718,19 +681,18 @@
     dma = pltpu.SemaphoreType.DMA
     return pl.pallas_call(
         mix_kernel,
-        in_specs=[vmem, hbm],
+        in_specs=[vmem, vmem],
         out_specs=vmem,
         out_shape=jax.ShapeDtypeStruct((rows, cols), bf16),
         scratch_shapes=[
-            pltpu.VMEM((4, width, cols), bf16),
             pltpu.VMEM((4, rows, cols), bf16),
             pltpu.VMEM((2, rows, cols), bf16),
             pltpu.VMEM((rows, cols), bf16),
-            dma((4,)), dma((2, PIECES)), dma((2, PIECES)), dma((PIECES,)), dma((PIECES,)),
+            dma((2, PIECES)), dma((2, PIECES)), dma((PIECES,)), dma((PIECES,)),
         ],
-        compiler_params=pltpu.CompilerParams(has_side_effects=True, collective_id=1, vmem_limit_bytes=56 * 2**20),
+        compiler_params=pltpu.CompilerParams(has_side_effects=True, collective_id=1, vmem_limit_bytes=LIMIT),
         name="mix",
-    )(flat, final)
+    )(local(flat), local(final))
 
 
 def on_device(

time: 125 us -> 112 us (0.90)
  the two profiles are of different devices: /device:TPU:9 before, /device:TPU:0 now
where the time goes in v3:
time: 112 us
  Pallas kernels  108 us (96%)
  local copies, waits for them, and re-layouts  2.55 us (2%)
    pallas_call x1, Pallas kernels, project(): pl.pallas_call(project_kernel, in_specs=[hbm] * 15, out_specs=[vmem] * 4,...  85.1 us
    pallas_call x1, Pallas kernels, mix(): pl.pallas_call(mix_kernel, in_specs=[vmem, vmem], out_specs=vmem, out_sha...  13.3 us
    pallas_call x1, Pallas kernels, attend(): pl.pallas_call(functools.partial(attend_kernel, heads, features), in_spec...  10 us

profile of v3, /device:TPU:0, one launch (start us, length us, event | category | flops | bytes accessed | tf_op | source)
XLA Modules:
  0.0 111.6 jit_solution(8151270914264122378)
XLA Ops:
  0.6 1.8 %copy_bitcast_fusion = (bf16[192,512]{1,0:T(8,128)(2,1)}, bf16[192,512]{1,0:T(8,128)(2,1)}) fusion(bf16[24,8,4,128]{3,2,1,0:T(4,128)(2,1)} %bitcast.24, bf16[24,8,4,128]{3,2,1,0:T(4,128)(2,1)} %bitcast.25), kind=kLoop, calls=%fused_computation | loop fusion | bytes 786432 | tf_op jit(solution)/shard_map/reshape | solution.py:733
  2.4 85.1 %project.1 = (f32[4,192,512]{2,1,0:T(8,128)S(1)}, f32[16,192]{1,0:T(8,128)S(1)}, f32[48,4,128,128]{3,2,1,0:T(8,128)S(1)}, bf16[4,512,1024]{2,1,0:T(8,128)(2,1)S(1)}) custom-call(bf16[192,1024]{1,0:T(8,128)(2,1)} %x_hbm.1, f32[4,1,1024]{2,1,0:T(1,128)} %bitcast.28, bf16[192,512]{1,0:T(8,128)(2,1)} %get-tuple-element.15.keys_hbm, ...), custom_call_target="tpu_custom_call" | custom-call | tf_op jit(solution)/shard_map/project/pallas_call | solution.py:584
  87.5 10.0 %attend.1 = (bf16[192,512]{1,0:T(8,128)(2,1)S(1)}, f32[48,4,128,128]{3,2,1,0:T(8,128)}) custom-call(f32[16,192]{1,0:T(8,128)S(1)} %get-tuple-element.8.few_ref, f32[16,48]{1,0:T(8,128)} %bitcast.32, f32[1,4]{1,0:T(1,128)} %bitcast.33, f32[1,4]{1,0:T(1,128)} %bitcast.34, f32[1,128]{1,0:T(1,128)} %bitcast.35, f32[4,192,512]{2,1,0:T(8,128)S(1)} %get-tuple-element.9.parts, ...), custom_call_target="tpu_custom_call" | custom-call | flops 5000000000 | bytes 12582912 | tf_op jit(solution)/shard_map/attend/pallas_call | solution.py:201
  97.6 13.3 %mix.1 = bf16[192,1024]{1,0:T(8,128)(2,1)S(1)} custom-call(bf16[192,512]{1,0:T(8,128)(2,1)S(1)} %get-tuple-element.11.flat_ref, bf16[4,512,1024]{2,1,0:T(8,128)(2,1)S(1)} %get-tuple-element.12.f_ref), custom_call_target="tpu_custom_call" | custom-call | tf_op jit(solution)/shard_map/mix/pallas_call | solution.py:682
  110.9 0.7 copy.26

commit v4 on v3

--- a/solution.py
+++ b/solution.py
@@ -100,74 +100,136 @@
                 o_ref[seq, h] = c_scr[pl.ds(h * SB + seq, 1), :] * s_ref[seq, h] + add
 
 
-def attend_kernel(heads, features, few_ref, extra_ref, rate_ref, offset_ref, w_ref, parts, state, o_ref, kept, thin, rk, rq, qf, kf, vf, zf, of, done):
-    keep = pltpu.make_async_copy(state, kept, done)
-    keep.start()
-    rows = o_ref.shape[0]
-    blocks = state.shape[0] // SB
-    few = rows_to_columns(few_ref[...])
+def attend_items(items, scratch, load, factor, state_at, scalars, gain, emit):
+    rk, rq, qf, kf, vf, zf, of = scratch
+    low = first_half()
+    for j, item in enumerate(items):
+        for n, dst in enumerate((qf, kf, vf, zf)):
+            dst[pl.ds(j * TALL, TALL), :] = (load(item, n) * factor(item)).astype(bf16).astype(f32)
+    for pair in range(SB // 2):
+        for j, item in enumerate(items):
+            at = tile(j, pair)
+            lhs = jnp.concatenate([kf[at, :], qf[at, :]], axis=0).astype(bf16)
+            r0 = jnp.dot(lhs, state_at(item, 2 * pair).astype(bf16), preferred_element_type=f32)
+            r1 = jnp.dot(lhs, state_at(item, 2 * pair + 1).astype(bf16), preferred_element_type=f32)
+            rk[at, :] = jnp.where(low, r0[:8], r1[:8])
+            rq[at, :] = jnp.where(low, r0[8:], r1[8:])
+    for j, item in enumerate(items):
+        scale = jnp.ones((SB, 1), f32)
+        ks, us, norms = [], [], []
+        for p in range(P_SIZE):
+            at = proposal(j, p)
+            g, strength = scalars(item, p)
+            key = kf[at, :]
+            query = qf[at, :]
+            norm = lax.rsqrt(lane_dot(key, key) + epsilon)
+            qnorm = lax.rsqrt(lane_dot(query, query) + epsilon) * DK ** (-0.5)
+            rec = (scale * norm) * rk[at, :]
+            for ki, ui, ni in zip(ks, us, norms):
+                rec = rec + (lane_dot(ki, key) * (ni * norm)) * ui
+            us = [ui * g for ui in us]
+            scale = scale * g
+            us.append(strength * (vf[at, :] - g * rec))
+            ks.append(key)
+            norms.append(norm)
+            att = (scale * qnorm) * rq[at, :]
+            for ki, ui, ni in zip(ks, us, norms):
+                att = att + (lane_dot(ki, query) * (ni * qnorm)) * ui
+            gate = zf[at, :]
+            mean = jnp.sum(att * att, axis=-1, keepdims=True) / DK
+            of[at, :] = att * lax.rsqrt(mean + epsilon) * gain * (gate * jax.nn.sigmoid(gate))
+    for j, item in enumerate(items):
+        emit(item, of[pl.ds(j * TALL, TALL), :].astype(bf16))
+
+
+def small_terms(heads, features, few_wide, extra, rates, offset, thin):
+    rows = few_wide.shape[1]
+    few = rows_to_columns(few_wide)
     factor = lax.rsqrt(few[:, 2 * heads : 2 * heads + 1] / features + epsilon)
-    seqs = extra_ref.shape[1]
+    seqs = extra.shape[1]
     row = lax.broadcasted_iota(jnp.int32, (rows, seqs), 0)
     owner = jnp.right_shift(row, 2) == lax.broadcasted_iota(jnp.int32, (rows, seqs), 1)
     spread = lax.dot_general(
-        owner.astype(f32), extra_ref[...], (((1,), (1,)), ((), ())),
+        owner.astype(f32), extra, (((1,), (1,)), ((), ())),
         precision=lax.Precision.HIGHEST, preferred_element_type=f32,
     )
     turn = jnp.bitwise_and(lax.broadcasted_iota(jnp.int32, (rows, heads), 0), 3)
-    extra = pick(turn, [spread[:, p * heads : (p + 1) * heads] for p in range(P_SIZE)])
-    raised = few[:, :heads] * factor + offset_ref[...]
+    struck = pick(turn, [spread[:, p * heads : (p + 1) * heads] for p in range(P_SIZE)])
+    raised = few[:, :heads] * factor + offset
     soft = jnp.maximum(raised, 0.0) + jnp.log1p(jnp.exp(-jnp.abs(raised)))
-    thin[:, :heads] = jnp.exp(extra - jnp.exp(rate_ref[...]) * soft)
+    thin[:, :heads] = jnp.exp(struck - jnp.exp(rates) * soft)
     thin[:, heads : 2 * heads] = jax.nn.sigmoid(few[:, heads : 2 * heads] * factor)
     thin[:, 2 * heads : 2 * heads + 1] = factor
-    low = first_half()
-    gain = w_ref[...]
+
+
+def attend_kernel(heads, features, few_ref, extra_ref, rate_ref, offset_ref, w_ref, parts, state, o_ref, kept, thin, *rest):
+    scratch, done = rest[:-1], rest[-1]
+    keep = pltpu.make_async_copy(state, kept, done)
+    keep.start()
+    small_terms(heads, features, few_ref[...], extra_ref[...], rate_ref[...], offset_ref[...], thin)
 
     def block(i, carry):
         base = i * TALL
         tall = pl.ds(base, TALL)
-        scaling = thin[tall, 2 * heads : 2 * heads + 1]
-        for n, dst in enumerate((qf, kf, vf, zf)):
-            load_heads(heads, parts.at[n, tall], dst, scaling)
-        for pair in range(SB // 2):
-            for h in range(heads):
-                at = tile(h, pair)
-                lhs = jnp.concatenate([kf[at, :], qf[at, :]], axis=0).astype(bf16)
-                r0 = jnp.dot(lhs, state[i * SB + 2 * pair, h].astype(bf16), preferred_element_type=f32)
-                r1 = jnp.dot(lhs, state[i * SB + 2 * pair + 1, h].astype(bf16), preferred_element_type=f32)
-                rk[at, :] = jnp.where(low, r0[:8], r1[:8])
-                rq[at, :] = jnp.where(low, r0[8:], r1[8:])
-        for h in range(heads):
-            scale = jnp.ones((SB, 1), f32)
-            ks, us, norms = [], [], []
-            for p in range(P_SIZE):
-                at = proposal(h, p)
-                scalars = thin[pl.ds(base + p, SB, stride=P_SIZE), :]
-                key = kf[at, :]
-                query = qf[at, :]
-                norm = lax.rsqrt(lane_dot(key, key) + epsilon)
-                qnorm = lax.rsqrt(lane_dot(query, query) + epsilon) * DK ** (-0.5)
-                g = scalars[:, h : h + 1]
-                rec = (scale * norm) * rk[at, :]
-                for ki, ui, ni in zip(ks, us, norms):
-                    rec = rec + (lane_dot(ki, key) * (ni * norm)) * ui
-                us = [ui * g for ui in us]
-                scale = scale * g
-                us.append(scalars[:, heads + h : heads + h + 1] * (vf[at, :] - g * rec))
-                ks.append(key)
-                norms.append(norm)
-                att = (scale * qnorm) * rq[at, :]
-                for ki, ui, ni in zip(ks, us, norms):
-                    att = att + (lane_dot(ki, query) * (ni * qnorm)) * ui
-                gate = zf[at, :]
-                mean = jnp.sum(att * att, axis=-1, keepdims=True) / DK
-                of[at, :] = att * lax.rsqrt(mean + epsilon) * gain * (gate * jax.nn.sigmoid(gate))
-        for h in range(heads):
-            o_ref[tall, h * DK : (h + 1) * DK] = of[pl.ds(h * TALL, TALL), :].astype(bf16)
+
+        def scalars(h, p):
+            both = thin[pl.ds(base + p, SB, stride=P_SIZE), :]
+            return both[:, h : h + 1], both[:, heads + h : heads + h + 1]
+
+        def emit(h, value):
+            o_ref[tall, h * DK : (h + 1) * DK] = value
+
+        attend_items(
+            range(heads), scratch,
+            lambda h, n: parts[n, tall, h * DK : (h + 1) * DK],
+            lambda h: thin[tall, 2 * heads : 2 * heads + 1],
+            lambda h, seq: state[i * SB + seq, h],
+            scalars, w_ref[...], emit,
+        )
         return carry
 
-    lax.fori_loop(0, blocks, block, 0)
+    lax.fori_loop(0, state.shape[0] // SB, block, 0)
+    keep.wait()
+
+
+GROUP = 3
+
+
+def attend_head(h, heads, blocks, scratch, parts_at, thin, state, gain, flat):
+    def group(it, carry):
+        def tall(j):
+            return pl.ds((it * GROUP + j) * TALL, TALL)
+
+        def scalars(j, p):
+            both = thin[pl.ds((it * GROUP + j) * TALL + p, SB, stride=P_SIZE), :]
+            return tuple(pick(h, [both[:, n + m : n + m + 1] for m in range(heads)]) for n in (0, heads))
+
+        def emit(j, value):
+            flat[tall(j), pl.ds(pl.multiple_of(h * DK, DK), DK)] = value
+
+        attend_items(
+            range(GROUP), scratch,
+            lambda j, n: parts_at(tall(j), n),
+            lambda j: thin[tall(j), 2 * heads : 2 * heads + 1],
+            lambda j, seq: state[(it * GROUP + j) * SB + seq, h],
+            scalars, gain, emit,
+        )
+        return carry
+
+    lax.fori_loop(0, blocks // GROUP, group, 0)
+
+
+def last_kernel(heads, thin, w_ref, parts, state, some, columns, o_ref, kept, flat, *rest):
+    scratch, done = rest[:-1], rest[-1]
+    keep = pltpu.make_async_copy(state, kept, done)
+    keep.start()
+    flat[...] = some[...]
+    blocks = state.shape[0] // SB
+    attend_head(
+        heads - 1, heads, blocks, scratch, lambda at, n: parts[at, n * DK : (n + 1) * DK], thin, state, w_ref[...], flat
+    )
+    for c in range(columns.shape[0]):
+        o_ref[c] = jnp.dot(flat[...], columns[c], preferred_element_type=f32).astype(bf16)
     keep.wait()
 
 
@@ -224,18 +286,42 @@
     return chosen
 
 
+def last_head(thin, gain, parts, state, some, columns):
+    seqs, heads = state.shape[:2]
+    rows, width = some.shape
+    vmem = pl.BlockSpec(memory_space=pltpu.VMEM)
+    return pl.pallas_call(
+        functools.partial(last_kernel, heads),
+        in_specs=[vmem] * 6,
+        out_specs=[vmem, pl.BlockSpec(memory_space=pl.ANY)],
+        out_shape=[
+            pltpu.VMEM((columns.shape[0], rows, columns.shape[2]), bf16),
+            jax.ShapeDtypeStruct(state.shape, f32),
+        ],
+        scratch_shapes=[
+            pltpu.VMEM((rows, width), bf16),
+            *[pltpu.VMEM((GROUP * TALL, DK), f32)] * 7,
+            pltpu.SemaphoreType.DMA,
+        ],
+        compiler_params=pltpu.CompilerParams(vmem_limit_bytes=LIMIT),
+        cost_estimate=pl.CostEstimate(flops=5_000_000_000, bytes_accessed=state.size * 4, transcendentals=0),
+        name="last_head",
+    )(local(thin), gain.reshape(1, DK), local(parts), local(state), local(some), local(columns))
+
+
 def turned_slot(t):
     return pick(t, (0, 2, 1, 3))
 
 
-def project_kernel(x_hbm, gain_hbm, keys_hbm, values_hbm, fade_hbm, pull_hbm, count_hbm, wf, ws, wq, wk, wv, wz, wo,
-                   state, acc, few_ref, taken, fbuf,
-                   x_ref, gain_ref, keys, values, fade, pull, counts, fs, thin,
+def project_kernel(x_hbm, gain_hbm, keys_hbm, values_hbm, fade_hbm, pull_hbm, count_hbm, extra_hbm, rate_hbm, offset_hbm,
+                   outer_hbm, wf, ws, wq, wk, wv, wz, wo, state, last, small, taken, fbuf, flat,
+                   x_ref, gain_ref, keys, values, fade, pull, counts, extra, rates, offset, outer, fs, thin, few_ref, acc,
                    xpre, xbuf, gbuf, w, sbuf, abuf, bbuf, cbuf, esend, erecv, s_in,
-                   r_scr, u_scr, c_scr, kf, vf,
+                   r_scr, u_scr, c_scr, kf, vf, a0, a1, a2, a3, a4, a5, a6,
                    lsem, xs, xp, xr, wsem, ss, ar, br, cr, es, er, ins, fsem, fss, fzr, fys, fyr):
     k, t, g = lax.axis_index("kv"), lax.axis_index("tp"), lax.axis_index("grp")
     depth, width = w.shape[1], w.shape[2]
+    features = gain_ref.shape[0] * depth
     rows = x_ref.shape[0]
     blocks = state.shape[0] // SB
     heads = state.shape[1]
@@ -251,7 +337,8 @@
         for n, (src, dst) in enumerate(
             (
                 (x_hbm, x_ref), (gain_hbm, gain_ref), (keys_hbm, keys), (values_hbm, values), (fade_hbm, fade),
-                (pull_hbm, pull), (count_hbm, counts), (wf.at[:, here], fs.at[0]), (ws.at[:, here], fs.at[1]),
+                (pull_hbm, pull), (count_hbm, counts), (extra_hbm, extra), (rate_hbm, rates), (offset_hbm, offset), (outer_hbm, outer),
+                (wf.at[:, here], fs.at[0]), (ws.at[:, here], fs.at[1]),
             )
         )
     ]
@@ -259,7 +346,13 @@
         load.start()
     f_load = pltpu.make_async_copy(wo, fbuf.at[k], fsem)
     f_load.start()
-    loads = [pltpu.make_async_copy(src, w.at[i], wsem.at[i]) for i, src in enumerate((wq, wk, wv, wz))]
+    loads = [
+        pltpu.make_async_copy(
+            src.at[:, pl.ds(h * DK, DK)], w.at[h, :, pl.ds(n * DK, DK)], wsem.at[h * 4 + n]
+        )
+        for h in range(heads)
+        for n, src in enumerate((wq, wk, wv, wz))
+    ]
     for load in loads:
         load.start()
 
@@ -454,55 +547,91 @@
             r_scr, u_scr, c_scr, kf, vf,
         )
 
+    def accept_all():
+        def one(i, carry):
+            accept(i)
+            return carry
+
+        lax.fori_loop(0, blocks, one, 0)
+
+    chunk_head, chunk_stage = (0, 1, 0, 0, 2, 1, 1, 3, 2, 3, 2, 3), (0, 0, 1, 2, 0, 1, 2, 0, 1, 1, 2, 2)
+    prepared = (3 - end, end, 3 - near, near)
+
+    def settle_small():
+        few_ref[...] = esend[k]
+        for src in range(4):
+
+            @pl.when(k != src)
+            def _():
+                remote(esend.at[src], erecv.at[src], es.at[src], er.at[src], k, beside).wait()
+                few_ref[...] += erecv[src]
+
+        small_terms(heads, features, few_ref[...], extra[...], rates[...], offset[...], small)
+
+    def attention(h):
+        attend_head(
+            h, heads, blocks, (a0, a1, a2, a3, a4, a5, a6),
+            lambda at, n: acc[h, at, n * DK : (n + 1) * DK], small, taken, outer[...], flat,
+        )
+
+    @pl.when(inside)
+    def _():
+        def one(i, carry):
+            prepare(pick(i, prepared))
+            return carry
+
+        lax.fori_loop(0, 4, one, 0)
+        f_take(f_order[0])
+        f_take(f_order[1])
+        accept_all()
+
     def step(i, carry):
-        stage, c = i // 4, i % 4
+        h, stage = pick(i, chunk_head), pick(i, chunk_stage)
         r = pick(stage, (3 - end, 3 - near, near))
 
-        @pl.when(c == 0)
-        def _():
-            prepare(r)
-
-        @pl.when(i == 2)
-        def _():
-            prepare(end)
+        @pl.when(jnp.logical_and(is_end, i < 4))
+        def _():
+            prepare(pick(i, prepared))
 
         @pl.when(is_end)
         def _():
-            sbuf[i] = product(r, c).astype(bf16)
+            sbuf[i] = product(r, h).astype(bf16)
             remote(sbuf.at[i], abuf.at[i], ss.at[i], ar.at[i], near, t).start()
 
-        @pl.when(jnp.logical_and(inside, i == 1))
-        def _():
-            f_take(f_order[0])
-            f_take(f_order[1])
-
-        @pl.when(jnp.logical_and(inside, i == 5))
-        def _():
-            f_take(f_order[2])
-
-        @pl.when(jnp.logical_and(is_end, i == 4))
-        def _():
-            f_take(f_order[0])
-
-        @pl.when(jnp.logical_and(inside, i < 8))
-        def _():
-            part = product(r, c)
+        @pl.when(jnp.logical_and(inside, stage < 2))
+        def _():
+            part = product(r, h)
             sbuf[i] = (part + from_end(i)).astype(bf16)
             remote(sbuf.at[i], bbuf.at[i], ss.at[i], br.at[i], 3 - near, t).start()
 
-        @pl.when(jnp.logical_and(inside, stage == 1))
-        def _():
-            part = product(end, c)
-            sbuf[8 + c] = (part + from_inner(c)).astype(bf16)
-            remote(sbuf.at[8 + c], cbuf.at[c], ss.at[8 + c], cr.at[c], end, t).start()
-
-        @pl.when(jnp.logical_and(inside, stage == 2))
-        def _():
-            acc[c] = product(r, c) + from_inner(4 + c) + from_end(i)
-
-        @pl.when(i % 2 == 0)
-        def _():
-            accept(i // 2)
+        @pl.when(jnp.logical_and(inside, i == 2))
+        def _():
+            f_take(f_order[2])
+
+        back = jnp.logical_or(jnp.logical_or(i == 2, i == 3), jnp.logical_or(i == 6, i == 9))
+
+        @pl.when(jnp.logical_and(inside, back))
+        def _():
+            m = jnp.where(i == 2, 0, i // 3)
+            part = product(end, m)
+            sbuf[12 + m] = (part + from_inner(pick(m, (0, 1, 4, 7)))).astype(bf16)
+            remote(sbuf.at[12 + m], cbuf.at[m], ss.at[12 + m], cr.at[m], end, t).start()
+
+        @pl.when(jnp.logical_and(inside, i == 4))
+        def _():
+            settle_small()
+
+        ready = jnp.logical_or(jnp.logical_or(i == 4, i == 7), i == 10)
+
+        @pl.when(jnp.logical_and(inside, ready))
+        def _():
+            m = i // 3 - 1
+            acc[m] = product(near, m) + from_inner(pick(m, (2, 5, 8))) + from_end(pick(m, (3, 6, 10)))
+            attention(m)
+
+        @pl.when(jnp.logical_and(inside, i == 11))
+        def _():
+            last[...] = product(near, 3) + from_inner(9) + from_end(11)
 
         return carry
 
@@ -510,28 +639,33 @@
 
     @pl.when(is_end)
     def _():
+        f_take(f_order[0])
+        accept_all()
+        settle_small()
         f_take(f_order[1])
 
-        def finish(c, carry):
-            part = product(end, c)
-
-            @pl.when(c == 1)
+        def returned(m):
+            part = product(end, m)
+            remote(cbuf.at[m], cbuf.at[m], ss.at[m], cr.at[m], k, beside).wait_recv()
+            return part + cbuf[m].astype(f32)
+
+        def finish(m, carry):
+            acc[m] = returned(m)
+            attention(m)
+
+            @pl.when(m == 1)
             def _():
                 f_take(f_order[2])
 
-            remote(cbuf.at[c], cbuf.at[c], ss.at[c], cr.at[c], k, beside).wait_recv()
-            acc[c] = part + cbuf[c].astype(f32)
             return carry
 
-        lax.fori_loop(0, 4, finish, 0)
-
-    few_ref[...] = esend[k]
+        lax.fori_loop(0, 3, finish, 0)
+        last[...] = returned(3)
+
     for src in range(4):
 
         @pl.when(k != src)
         def _():
-            remote(esend.at[src], erecv.at[src], es.at[src], er.at[src], k, beside).wait()
-            few_ref[...] += erecv[src]
             remote(fbuf.at[src, half], fbuf.at[src, half], fys.at[src], fyr.at[src], k, beside).wait()
 
     remote(x_ref.at[bottom], xpre, xs.at[0], xp, k, across).wait_send()
@@ -562,10 +696,19 @@
             f_pass(src, k, src).wait_send()
 
     for i in range(12):
-        remote(sbuf.at[i], abuf.at[i], ss.at[i], ar.at[i], k, beside).wait_send()
-
-
-def project(x, gain, weights, forgetting, strength, final, state, keys, values, fade, pull, counts):
+
+        @pl.when(is_end if chunk_stage[i] == 2 else k >= 0)
+        def _():
+            remote(sbuf.at[i], abuf.at[i], ss.at[i], ar.at[i], k, beside).wait_send()
+
+    for m in range(4):
+
+        @pl.when(inside)
+        def _():
+            remote(sbuf.at[12 + m], cbuf.at[m], ss.at[12 + m], cr.at[m], end, t).wait_send()
+
+
+def project(x, gain, weights, forgetting, strength, final, state, keys, values, fade, pull, counts, extra, rates, offset, outer):
     rows, depth = x.shape
     width = weights[0].shape[1]
     seqs, heads = state.shape[:2]
@@ -573,6 +716,7 @@
     vmem, hbm = pl.BlockSpec(memory_space=pltpu.VMEM), pl.BlockSpec(memory_space=pl.ANY)
     dma = pltpu.SemaphoreType.DMA
     gain = gain.reshape(-1, 1, depth)
+    rates, offset, outer = rates.reshape(1, heads), offset.reshape(1, heads), outer.reshape(1, DK)
     forgetting, strength = forgetting.T, strength.T
 
     def chunks(n):
@@ -583,45 +727,50 @@
 
     return pl.pallas_call(
         project_kernel,
-        in_specs=[hbm] * 15,
-        out_specs=[vmem] * 4,
+        in_specs=[hbm] * 19,
+        out_specs=[vmem] * 5,
         out_shape=[
-            pltpu.VMEM((4, rows, width), f32),
-            pltpu.VMEM((few_rows, rows), f32),
+            pltpu.VMEM((rows, width), f32),
+            pltpu.VMEM((rows, few_rows), f32),
             pltpu.VMEM(state.shape, f32),
             pltpu.VMEM((4,) + final.shape, bf16),
+            pltpu.VMEM((rows, width), bf16),
         ],
         scratch_shapes=[
             like(x), like(gain), like(keys), like(values), like(fade), like(pull), like(counts),
+            like(extra), like(rates), like(offset), like(outer),
             pltpu.VMEM((2, forgetting.shape[0], depth), bf16),
             pltpu.VMEM((seqs, 2 * P_SIZE * heads + 8), f32),
+            pltpu.VMEM((few_rows, rows), f32),
+            pltpu.VMEM((3, rows, width), f32),
             pltpu.VMEM((rows // 2, depth), bf16),
             pltpu.VMEM((4, rows, depth), bf16),
             pltpu.VMEM((4, rows, depth), bf16),
             pltpu.VMEM((4, depth, width), bf16),
-            chunks(12), chunks(12), chunks(8), chunks(4),
+            chunks(16), chunks(12), chunks(12), chunks(4),
             pltpu.VMEM((4, few_rows, rows), f32),
             pltpu.VMEM((4, few_rows, rows), f32),
             pltpu.VMEM((2, SB) + state.shape[1:], f32),
             *[pltpu.VMEM((heads * n, DK), f32) for n in (TALL, TALL, SB, TALL, TALL)],
-            dma((9,)), dma((9,)), dma, dma((4, 2)), dma((4,)), dma((12,)), dma((12,)), dma((8,)), dma((4,)), dma((4,)),
+            *[pltpu.VMEM((GROUP * TALL, DK), f32)] * 7,
+            dma((13,)), dma((9,)), dma, dma((4, 2)), dma((16,)), dma((16,)), dma((12,)), dma((12,)), dma((4,)), dma((4,)),
             dma((4,)), dma((2,)), dma, dma((6,)), dma((4,)), dma((4,)), dma((4,)),
         ],
         compiler_params=pltpu.CompilerParams(has_side_effects=True, collective_id=0, vmem_limit_bytes=LIMIT),
         name="project",
-    )(x, gain, keys, values, fade, pull, counts, forgetting, strength, *weights, final, state)
+    )(x, gain, keys, values, fade, pull, counts, extra, rates, offset, outer, forgetting, strength, *weights, final, state)
 
 
 PIECES = 3
 
 
-def mix_kernel(flat_ref, f_ref, o_ref, part, mate, cross, ms, mr, xs, xr):
+def mix_kernel(part, o_ref, mate, sent, cross, ms, mr, xs, xr):
     k, t, g = lax.axis_index("kv"), lax.axis_index("tp"), lax.axis_index("grp")
-    rows = flat_ref.shape[0]
+    rows = part.shape[1]
     piece = rows // PIECES
     beside = t + 1 - 2 * (t % 2)
     across = (t + 2) % 4
-    order = ((beside + 2) % 4, across, beside, t)
+    order = ((beside + 2) % 4, beside)
 
     def remote(src, dst, send, recv, tp):
         return pltpu.make_async_remote_copy(
@@ -637,36 +786,26 @@
 
     def to_mate(n, s):
         at = pl.ds(s * piece, piece)
-        return remote(part.at[2 * n, at], mate.at[n, at], ms.at[n, s], mr.at[n, s], beside)
+        return remote(part.at[order[n], at], mate.at[n, at], ms.at[n, s], mr.at[n, s], beside)
 
     def to_cross(s):
         at = pl.ds(s * piece, piece)
-        return remote(part.at[1, at], cross.at[at], xs.at[s], xr.at[s], across)
-
-    def fill(n, s):
-        at = pl.ds(s * piece, piece)
-        return jnp.dot(flat_ref[at, :], f_ref[order[n]], preferred_element_type=f32).astype(bf16)
-
-    for s in range(PIECES):
-        part[0, s * piece : (s + 1) * piece, :] = fill(0, s)
-        to_mate(0, s).start()
+        return remote(sent.at[at], cross.at[at], xs.at[s], xr.at[s], across)
+
+    for n in range(2):
+        for s in range(PIECES):
+            to_mate(n, s).start()
     for s in range(PIECES):
         at = slice(s * piece, (s + 1) * piece)
-        mine = fill(1, s).astype(f32)
         to_mate(0, s).wait_recv()
-        part[1, at, :] = (mine + mate[0, at, :].astype(f32)).astype(bf16)
+        sent[at, :] = (part[across, at, :].astype(f32) + mate[0, at, :].astype(f32)).astype(bf16)
         to_cross(s).start()
-    for s in range(PIECES):
-        part[2, s * piece : (s + 1) * piece, :] = fill(2, s)
-        to_mate(1, s).start()
-    for s in range(PIECES):
-        part[3, s * piece : (s + 1) * piece, :] = fill(3, s)
     for s in range(PIECES):
         at = slice(s * piece, (s + 1) * piece)
         to_mate(1, s).wait_recv()
         to_cross(s).wait_recv()
         o_ref[at, :] = (
-            part[3, at, :].astype(f32) + mate[1, at, :].astype(f32) + cross[at, :].astype(f32)
+            part[t, at, :].astype(f32) + mate[1, at, :].astype(f32) + cross[at, :].astype(f32)
         ).astype(bf16)
     for s in range(PIECES):
         to_mate(0, s).wait_send()
@@ -674,25 +813,24 @@
         to_cross(s).wait_send()
 
 
-def mix(flat, final):
-    rows, width = flat.shape
-    cols = final.shape[2]
-    vmem, hbm = pl.BlockSpec(memory_space=pltpu.VMEM), pl.BlockSpec(memory_space=pl.ANY)
+def mix(part):
+    rows, cols = part.shape[1:]
+    vmem = pl.BlockSpec(memory_space=pltpu.VMEM)
     dma = pltpu.SemaphoreType.DMA
     return pl.pallas_call(
         mix_kernel,
-        in_specs=[vmem, vmem],
+        in_specs=[vmem],
         out_specs=vmem,
         out_shape=jax.ShapeDtypeStruct((rows, cols), bf16),
         scratch_shapes=[
-            pltpu.VMEM((4, rows, cols), bf16),
             pltpu.VMEM((2, rows, cols), bf16),
+            pltpu.VMEM((rows, cols), bf16),
             pltpu.VMEM((rows, cols), bf16),
             dma((2, PIECES)), dma((2, PIECES)), dma((PIECES,)), dma((PIECES,)),
         ],
         compiler_params=pltpu.CompilerParams(has_side_effects=True, collective_id=1, vmem_limit_bytes=LIMIT),
         name="mix",
-    )(local(flat), local(final))
+    )(local(part))
 
 
 def on_device(
@@ -732,10 +870,13 @@
     fade, pull, extra = thin(earlier_forgetting), thin(earlier_strengths), thin(extra_forgetting)
     earlier = (memory_matrix, earlier_addresses.reshape(rows, width), earlier_contents.reshape(rows, width))
     if n_kv == 4 and n_tp == 4:
-        summed, few, taken, columns = project(
+        last, small, taken, columns, flat = project(
             candidate_embeddings, incoming_rms_scaling, weights, forgetting_projector, strength_projector_matrix,
-            final_projector, *earlier, fade, pull, admitted_counts.reshape(1, seqs),
-        )
+            final_projector, *earlier, fade, pull, admitted_counts.reshape(1, seqs), extra,
+            channel_forgetting_rates, forgetting_offset, outgoing_rms_scaling,
+        )
+        part, taken = last_head(small, outgoing_rms_scaling, last, taken, flat, columns)
+        mixed = mix(part)
     else:
         every = lax.all_gather(candidate_embeddings, "tp", axis=1, tiled=True)
         every = lax.all_to_all(every, "kv", split_axis=1, concat_axis=0, tiled=True)
@@ -757,12 +898,9 @@
         summed = lax.psum_scatter(partial, "kv", scatter_dimension=1, tiled=True).astype(f32)
         counts = admitted_counts.astype(f32).reshape(seqs, 1)
         taken = accepted(*earlier, jnp.concatenate([fade.T, pull.T, counts], axis=1))
-    flat, taken = attend(
-        features, taken, summed, few, extra, channel_forgetting_rates, forgetting_offset, outgoing_rms_scaling
-    )
-    if n_kv == 4 and n_tp == 4:
-        mixed = mix(flat, columns)
-    else:
+        flat, taken = attend(
+            features, taken, summed, few, extra, channel_forgetting_rates, forgetting_offset, outgoing_rms_scaling
+        )
         gathered = lax.all_gather(flat, "kv", axis=0, tiled=True)
         terms = jnp.dot(gathered, final_projector, preferred_element_type=f32).astype(bf16)
         terms = lax.all_to_all(terms, "kv", split_axis=0, concat_axis=1, tiled=True)

time: 112 us -> 108 us (0.964)
  the two profiles are of different devices: /device:TPU:0 before, /device:TPU:9 now
where the time goes in v4:
time: 108 us
  Pallas kernels  104 us (96%)
  local copies, waits for them, and re-layouts  2.55 us (2%)
    pallas_call x1, Pallas kernels, project(): pl.pallas_call(project_kernel, in_specs=[hbm] * 19, out_specs=[vmem] * 5,...  83 us
    pallas_call x1, Pallas kernels, mix(): pl.pallas_call(mix_kernel, in_specs=[vmem], out_specs=vmem, out_shape=jax...  16 us
    pallas_call x1, Pallas kernels, last_head(): pl.pallas_call(functools.partial(last_kernel, heads), in_specs=[vmem] * 6...  5.44 us

profile of v4, /device:TPU:9, one launch (start us, length us, event | category | flops | bytes accessed | tf_op | source)
XLA Modules:
  0.0 107.7 jit_solution(6732014686683757200)
XLA Ops:
  0.6 1.8 %copy_bitcast_fusion = (bf16[192,512]{1,0:T(8,128)(2,1)}, bf16[192,512]{1,0:T(8,128)(2,1)}) fusion(bf16[24,8,4,128]{3,2,1,0:T(4,128)(2,1)} %bitcast.24, bf16[24,8,4,128]{3,2,1,0:T(4,128)(2,1)} %bitcast.25), kind=kLoop, calls=%fused_computation | loop fusion | bytes 786432 | tf_op jit(solution)/shard_map/reshape | solution.py:871
  2.4 83.0 %project.1 = (f32[192,512]{1,0:T(8,128)S(1)}, f32[192,16]{1,0:T(8,128)S(1)}, f32[48,4,128,128]{3,2,1,0:T(8,128)S(1)}, bf16[4,512,1024]{2,1,0:T(8,128)(2,1)S(1)}, bf16[192,512]{1,0:T(8,128)(2,1)S(1)}) custom-call(bf16[192,1024]{1,0:T(8,128)(2,1)} %x_hbm.1, f32[4,1,1024]{2,1,0:T(1,128)} %bitcast.28, bf16[192,512]{1,0:T(8,128)(2,1)} %get-tuple-element.17.keys_hbm, ...), custom_call_target="tpu_custom_call" | custom-call | tf_op jit(solution)/shard_map/project/pallas_call | solution.py:728
  85.5 5.4 %last_head.1 = (bf16[4,192,1024]{2,1,0:T(8,128)(2,1)S(1)}, f32[48,4,128,128]{3,2,1,0:T(8,128)}) custom-call(f32[192,16]{1,0:T(8,128)S(1)} %get-tuple-element.9.thin, f32[1,128]{1,0:T(1,128)} %bitcast.36, f32[192,512]{1,0:T(8,128)S(1)} %get-tuple-element.10.parts, f32[48,4,128,128]{3,2,1,0:T(8,128)S(1)} %get-tuple-element.11.state, ...), custom_call_target="tpu_custom_call" | custom-call | flops 5000000000 | bytes 12582912 | tf_op jit(solution)/shard_map/last_head/pallas_call | solution.py:293
  90.9 16.0 %mix.1 = bf16[192,1024]{1,0:T(8,128)(2,1)S(1)} custom-call(bf16[4,192,1024]{2,1,0:T(8,128)(2,1)S(1)} %get-tuple-element.14.part), custom_call_target="tpu_custom_call" | custom-call | tf_op jit(solution)/shard_map/mix/pallas_call | solution.py:820
  106.9 0.7 copy.26

commit v5 on v4

--- a/solution.py
+++ b/solution.py
@@ -26,6 +26,11 @@
 
 
 def load_heads(heads, src, dst, factor=None):
+    if len(src.shape) == 4:
+        block = src[...].astype(f32)
+        for h in range(heads):
+            dst[pl.ds(h * TALL, TALL), :] = block[:, :, h, :].reshape(TALL, DK)
+        return
     for h in range(heads):
         part = src[:, h * DK : (h + 1) * DK].astype(f32)
         dst[pl.ds(h * TALL, TALL), :] = part if factor is None else (part * factor).astype(bf16).astype(f32)
@@ -202,10 +207,10 @@
 
         def scalars(j, p):
             both = thin[pl.ds((it * GROUP + j) * TALL + p, SB, stride=P_SIZE), :]
-            return tuple(pick(h, [both[:, n + m : n + m + 1] for m in range(heads)]) for n in (0, heads))
+            return both[:, h : h + 1], both[:, heads + h : heads + h + 1]
 
         def emit(j, value):
-            flat[tall(j), pl.ds(pl.multiple_of(h * DK, DK), DK)] = value
+            flat[tall(j), h * DK : (h + 1) * DK] = value
 
         attend_items(
             range(GROUP), scratch,
@@ -407,45 +412,63 @@
     def _():
         pl.semaphore_wait(barrier, 10)
 
-    half_tall = rows // 2
-    top, bottom = pl.ds(0, half_tall), pl.ds(half_tall, half_tall)
+    quarter = rows // 4
     locals_[0].wait()
 
+    def part(q):
+        return pl.ds(q * quarter, quarter)
+
+    def forward(q):
+        return remote(xpre.at[q], xbuf.at[k, part(2 + q)], xs.at[4 + q], xr.at[k, 2 + q], across, landing)
+
+    def outward(q):
+        return remote(x_ref.at[part(q)], xbuf.at[k, part(q)], xs.at[2 + q], xr.at[k, q], t, landing)
+
+    def settled_copy(q):
+        return pltpu.make_async_copy(x_ref.at[part(q)], xbuf.at[k, part(q)], xr.at[k, q])
+
+    def sideways(q):
+        return remote(x_ref.at[part(2 + q)], xpre.at[q], xs.at[q], xp.at[q], k, across)
+
     @pl.when(t == k)
     def _():
-        remote(x_ref.at[bottom], xbuf.at[k, bottom], xs.at[0], xr.at[k, 1], k, across).start()
-        pltpu.make_async_copy(x_ref.at[top], xbuf.at[k, top], xr.at[k, 0]).start()
+        for q in range(2):
+            remote(x_ref.at[part(2 + q)], xbuf.at[k, part(2 + q)], xs.at[q], xr.at[k, 2 + q], k, across).start()
+        for q in range(2):
+            settled_copy(q).start()
 
     @pl.when(t != k)
     def _():
-        remote(x_ref.at[bottom], xpre, xs.at[0], xp, k, across).start()
-        remote(x_ref.at[top], xbuf.at[k, top], xs.at[1], xr.at[k, 0], t, landing).start()
+        for q in range(2):
+            sideways(q).start()
+        for q in range(2):
+            outward(q).start()
 
     @pl.when(across != k)
     def _():
-        remote(xpre, xpre, xs.at[0], xp, k, across).wait_recv()
-        remote(xpre, xbuf.at[k, bottom], xs.at[2], xr.at[k, 1], across, landing).start()
+        for q in range(2):
+            sideways(q).wait_recv()
+            forward(q).start()
 
     kind = jnp.where(top_kind, 0, 1)
-    direct = pl.ds(kind * half_tall, half_tall)
-    crossed = pl.ds((1 - kind) * half_tall, half_tall)
-
-    def piece(r, at, send, kd, tp):
-        return remote(xbuf.at[r, at], xbuf.at[r, at], xs.at[send], xr.at[r, kd], k, tp)
-
-    def spread(r, n):
+
+    def piece(r, q, send, tp):
+        at = pl.ds(q * quarter, quarter)
+        return remote(xbuf.at[r, at], xbuf.at[r, at], xs.at[send], xr.at[r, q], k, tp)
+
+    def spread(r, n, q):
         settled = jnp.logical_and(t == k, r == k)
 
         @pl.when(settled)
         def _():
-            pltpu.make_async_copy(x_ref.at[top], xbuf.at[k, top], xr.at[k, 0]).wait()
+            settled_copy(q).wait()
 
         @pl.when(jnp.logical_not(settled))
         def _():
-            piece(r, direct, 3, kind, across).wait_recv()
-
-        piece(r, direct, 3 + n, kind, across).start()
-        piece(r, direct, 5 + n, kind, beside).start()
+            piece(r, 2 * kind + q, 6, across).wait_recv()
+
+        piece(r, 2 * kind + q, 6 + n, across).start()
+        piece(r, 2 * kind + q, 10 + n, beside).start()
 
     half_rows = fbuf.shape[1] // 2
     half = pl.ds(g * half_rows, half_rows)
@@ -456,8 +479,9 @@
     def f_swap(c):
         return remote(fbuf.at[c, half], fbuf.at[c, half], fys.at[c], fyr.at[c], k, t, 1 - g)
 
-    spread(near_src, 0)
-    spread(far_src, 1)
+    for q in range(2):
+        spread(near_src, 2 * q, q)
+        spread(far_src, 2 * q + 1, q)
     f_load.wait()
 
     @pl.when(k < 3)
@@ -468,9 +492,10 @@
     def _():
         f_pass(k, k - 1, 5).start()
 
-    for n, r in enumerate((near_src, far_src)):
-        piece(r, crossed, 3, 1 - kind, across).wait_recv()
-        piece(r, crossed, 7 + n, 1 - kind, beside).start()
+    for q in range(2):
+        for n, r in enumerate((near_src, far_src)):
+            piece(r, 2 - 2 * kind + q, 6, across).wait_recv()
+            piece(r, 2 - 2 * kind + q, 14 + 2 * q + n, beside).start()
 
     def f_forwards(c):
         return jnp.logical_or(jnp.logical_and(c < k, k < 3), jnp.logical_and(c > k, k > 0))
@@ -499,8 +524,8 @@
     for load in loads:
         load.wait()
     for r in (1 - corner, 3 - corner):
-        for kd in range(2):
-            piece(r, pl.ds(kd * half_tall, half_tall), 3, kd, beside).wait_recv()
+        for q in range(4):
+            piece(r, q, 6, beside).wait_recv()
 
     nt = (((1,), (1,)), ((), ()))
 
@@ -541,9 +566,9 @@
 
         fetch(i).wait()
 
-        tall, few_rows = pl.ds(i * TALL, TALL), pl.ds(i * SB, SB)
+        few_rows = pl.ds(i * SB, SB)
         accepted_kernel(
-            heads, s_in.at[i % 2], keys.at[tall], values.at[tall], thin.at[few_rows], taken.at[few_rows],
+            heads, s_in.at[i % 2], keys.at[few_rows], values.at[few_rows], thin.at[few_rows], taken.at[few_rows],
             r_scr, u_scr, c_scr, kf, vf,
         )
 
@@ -581,9 +606,9 @@
             return carry
 
         lax.fori_loop(0, 4, one, 0)
+        accept_all()
         f_take(f_order[0])
         f_take(f_order[1])
-        accept_all()
 
     def step(i, carry):
         h, stage = pick(i, chunk_head), pick(i, chunk_stage)
@@ -627,7 +652,12 @@
         def _():
             m = i // 3 - 1
             acc[m] = product(near, m) + from_inner(pick(m, (2, 5, 8))) + from_end(pick(m, (3, 6, 10)))
-            attention(m)
+
+        for m in range(3):
+
+            @pl.when(jnp.logical_and(inside, i == 4 + 3 * m))
+            def _():
+                attention(m)
 
         @pl.when(jnp.logical_and(inside, i == 11))
         def _():
@@ -649,17 +679,11 @@
             remote(cbuf.at[m], cbuf.at[m], ss.at[m], cr.at[m], k, beside).wait_recv()
             return part + cbuf[m].astype(f32)
 
-        def finish(m, carry):
+        for m in range(3):
             acc[m] = returned(m)
             attention(m)
-
-            @pl.when(m == 1)
-            def _():
+            if m == 1:
                 f_take(f_order[2])
-
-            return carry
-
-        lax.fori_loop(0, 3, finish, 0)
         last[...] = returned(3)
 
     for src in range(4):
@@ -668,18 +692,21 @@
         def _():
             remote(fbuf.at[src, half], fbuf.at[src, half], fys.at[src], fyr.at[src], k, beside).wait()
 
-    remote(x_ref.at[bottom], xpre, xs.at[0], xp, k, across).wait_send()
+    for q in range(2):
+        sideways(q).wait_send()
 
     @pl.when(t != k)
     def _():
-        remote(x_ref.at[top], xbuf.at[k, top], xs.at[1], xr.at[k, 0], t, landing).wait_send()
+        for q in range(2):
+            outward(q).wait_send()
 
     @pl.when(across != k)
     def _():
-        remote(xpre, xbuf.at[k, bottom], xs.at[2], xr.at[k, 1], across, landing).wait_send()
-
-    for n in range(6):
-        piece(k, top, 3 + n, 0, beside).wait_send()
+        for q in range(2):
+            forward(q).wait_send()
+
+    for n in range(12):
+        piece(k, 0, 6 + n, beside).wait_send()
 
     @pl.when(k < 3)
     def _():
@@ -743,7 +770,7 @@
             pltpu.VMEM((seqs, 2 * P_SIZE * heads + 8), f32),
             pltpu.VMEM((few_rows, rows), f32),
             pltpu.VMEM((3, rows, width), f32),
-            pltpu.VMEM((rows // 2, depth), bf16),
+            pltpu.VMEM((2, rows // 4, depth), bf16),
             pltpu.VMEM((4, rows, depth), bf16),
             pltpu.VMEM((4, rows, depth), bf16),
             pltpu.VMEM((4, depth, width), bf16),
@@ -753,7 +780,7 @@
             pltpu.VMEM((2, SB) + state.shape[1:], f32),
             *[pltpu.VMEM((heads * n, DK), f32) for n in (TALL, TALL, SB, TALL, TALL)],
             *[pltpu.VMEM((GROUP * TALL, DK), f32)] * 7,
-            dma((13,)), dma((9,)), dma, dma((4, 2)), dma((16,)), dma((16,)), dma((12,)), dma((12,)), dma((4,)), dma((4,)),
+            dma((13,)), dma((18,)), dma((2,)), dma((4, 4)), dma((16,)), dma((16,)), dma((12,)), dma((12,)), dma((4,)), dma((4,)),
             dma((4,)), dma((2,)), dma, dma((6,)), dma((4,)), dma((4,)), dma((4,)),
         ],
         compiler_params=pltpu.CompilerParams(has_side_effects=True, collective_id=0, vmem_limit_bytes=LIMIT),
@@ -868,11 +895,10 @@
 
     weights = (probe_projector, address_projector, content_projector, sigmoid_mask_matrix)
     fade, pull, extra = thin(earlier_forgetting), thin(earlier_strengths), thin(extra_forgetting)
-    earlier = (memory_matrix, earlier_addresses.reshape(rows, width), earlier_contents.reshape(rows, width))
     if n_kv == 4 and n_tp == 4:
         last, small, taken, columns, flat = project(
             candidate_embeddings, incoming_rms_scaling, weights, forgetting_projector, strength_projector_matrix,
-            final_projector, *earlier, fade, pull, admitted_counts.reshape(1, seqs), extra,
+            final_projector, memory_matrix, earlier_addresses, earlier_contents, fade, pull, admitted_counts.reshape(1, seqs), extra,
             channel_forgetting_rates, forgetting_offset, outgoing_rms_scaling,
         )
         part, taken = last_head(small, outgoing_rms_scaling, last, taken, flat, columns)
@@ -897,7 +923,8 @@
         partial = jnp.stack([jnp.dot(gained, w, preferred_element_type=f32).astype(bf16) for w in weights])
         summed = lax.psum_scatter(partial, "kv", scatter_dimension=1, tiled=True).astype(f32)
         counts = admitted_counts.astype(f32).reshape(seqs, 1)
-        taken = accepted(*earlier, jnp.concatenate([fade.T, pull.T, counts], axis=1))
+        keys, values = earlier_addresses.reshape(rows, width), earlier_contents.reshape(rows, width)
+        taken = accepted(memory_matrix, keys, values, jnp.concatenate([fade.T, pull.T, counts], axis=1))
         flat, taken = attend(
             features, taken, summed, few, extra, channel_forgetting_rates, forgetting_offset, outgoing_rms_scaling
         )

time: 108 us -> 103 us (0.954); the launches traced: 108 us -> 101 us
  Pallas kernels: 104 us -> 99.4 us
  local copies, waits for them, and re-layouts: 2.55 us -> 0.75 us
    pallas_call x1, Pallas kernels: 83 us -> 80.1 us  [project(): pl.pallas_call(project_kernel, in_specs=[hbm] * 19, out_specs=[vmem] * 5,...]
    pallas_call x1, Pallas kernels: 16 us -> 13.8 us  [mix(): pl.pallas_call(mix_kernel, in_specs=[vmem], out_specs=vmem, out_shape=jax...]
    reshape x1 -> x0, local copies, waits for them, and re-layouts: 1.8 us -> none  [on_device(): earlier_contents.reshape(rows, width)]
where the time goes in v5:
time: 103 us; the launch traced here: 101 us
  Pallas kernels  99.4 us (97%)
    pallas_call x1, Pallas kernels, project(): pl.pallas_call(project_kernel, in_specs=[hbm] * 19, out_specs=[vmem] * 5,...  80.1 us
    pallas_call x1, Pallas kernels, mix(): pl.pallas_call(mix_kernel, in_specs=[vmem], out_specs=vmem, out_shape=jax...  13.8 us
    pallas_call x1, Pallas kernels, last_head(): pl.pallas_call(functools.partial(last_kernel, heads), in_specs=[vmem] * 6...  5.44 us

profile of v5, /device:TPU:9, one launch (start us, length us, event | category | flops | bytes accessed | tf_op | source)
XLA Modules:
  0.0 100.8 jit_solution(12088044459359336815)
XLA Ops:
  0.6 80.1 %project.1 = (f32[192,512]{1,0:T(8,128)S(1)}, f32[192,16]{1,0:T(8,128)S(1)}, f32[48,4,128,128]{3,2,1,0:T(8,128)S(1)}, bf16[4,512,1024]{2,1,0:T(8,128)(2,1)S(1)}, bf16[192,512]{1,0:T(8,128)(2,1)S(1)}) custom-call(bf16[192,1024]{1,0:T(8,128)(2,1)} %x_hbm.1, f32[4,1,1024]{2,1,0:T(1,128)} %bitcast.18, bf16[48,4,4,128]{3,2,1,0:T(4,128)(2,1)} %keys_hbm.1, ...), custom_call_target="tpu_custom_call" | custom-call | tf_op jit(solution)/shard_map/project/pallas_call | solution.py:755
  80.8 5.4 %last_head.1 = (bf16[4,192,1024]{2,1,0:T(8,128)(2,1)S(1)}, f32[48,4,128,128]{3,2,1,0:T(8,128)}) custom-call(f32[192,16]{1,0:T(8,128)S(1)} %get-tuple-element.9.thin, f32[1,128]{1,0:T(1,128)} %bitcast.26, f32[192,512]{1,0:T(8,128)S(1)} %get-tuple-element.10.parts, f32[48,4,128,128]{3,2,1,0:T(8,128)S(1)} %get-tuple-element.11.state, ...), custom_call_target="tpu_custom_call" | custom-call | flops 5000000000 | bytes 12582912 | tf_op jit(solution)/shard_map/last_head/pallas_call | solution.py:298
  86.2 13.8 %mix.1 = bf16[192,1024]{1,0:T(8,128)(2,1)S(1)} custom-call(bf16[4,192,1024]{2,1,0:T(8,128)(2,1)S(1)} %get-tuple-element.14.part), custom_call_target="tpu_custom_call" | custom-call | tf_op jit(solution)/shard_map/mix/pallas_call | solution.py:847
  100.0 0.7 copy.22

commit v6 on v5

--- a/solution.py
+++ b/solution.py
@@ -450,70 +450,81 @@
             sideways(q).wait_recv()
             forward(q).start()
 
-    kind = jnp.where(top_kind, 0, 1)
-
-    def piece(r, q, send, tp):
-        at = pl.ds(q * quarter, quarter)
-        return remote(xbuf.at[r, at], xbuf.at[r, at], xs.at[send], xr.at[r, q], k, tp)
-
-    def spread(r, n, q):
-        settled = jnp.logical_and(t == k, r == k)
-
-        @pl.when(settled)
-        def _():
-            settled_copy(q).wait()
-
-        @pl.when(jnp.logical_not(settled))
-        def _():
-            piece(r, 2 * kind + q, 6, across).wait_recv()
-
-        piece(r, 2 * kind + q, 6 + n, across).start()
-        piece(r, 2 * kind + q, 10 + n, beside).start()
-
-    half_rows = fbuf.shape[1] // 2
-    half = pl.ds(g * half_rows, half_rows)
-
-    def f_pass(c, to, sem):
-        return remote(fbuf.at[c, half], fbuf.at[c, half], fss.at[sem], fzr.at[c], to, t)
-
-    def f_swap(c):
-        return remote(fbuf.at[c, half], fbuf.at[c, half], fys.at[c], fyr.at[c], k, t, 1 - g)
-
-    for q in range(2):
-        spread(near_src, 2 * q, q)
-        spread(far_src, 2 * q + 1, q)
-    f_load.wait()
-
-    @pl.when(k < 3)
-    def _():
-        f_pass(k, k + 1, 4).start()
-
-    @pl.when(k > 0)
-    def _():
-        f_pass(k, k - 1, 5).start()
-
-    for q in range(2):
-        for n, r in enumerate((near_src, far_src)):
-            piece(r, 2 - 2 * kind + q, 6, across).wait_recv()
-            piece(r, 2 - 2 * kind + q, 14 + 2 * q + n, beside).start()
-
-    def f_forwards(c):
-        return jnp.logical_or(jnp.logical_and(c < k, k < 3), jnp.logical_and(c > k, k > 0))
-
-    def f_take(c):
-        to = jnp.where(c < k, k + 1, k - 1)
-        f_pass(c, k, c).wait_recv()
-
-        @pl.when(f_forwards(c))
-        def _():
-            f_pass(c, to, c).start()
-
-        f_swap(c).start()
-
     end = jnp.where(k <= 1, 0, 3)
     near = jnp.where(k <= 1, 1, 2)
     is_end = k == end
     inside = jnp.logical_not(is_end)
+    kind = jnp.where(top_kind, 0, 1)
+
+    def piece(r, q, send, tp):
+        at = pl.ds(q * quarter, quarter)
+        return remote(xbuf.at[r, at], xbuf.at[r, at], xs.at[send], xr.at[r, q], k, tp)
+
+    def spread(r, n, q):
+        settled = jnp.logical_and(t == k, r == k)
+
+        @pl.when(settled)
+        def _():
+            settled_copy(q).wait()
+
+        @pl.when(jnp.logical_not(settled))
+        def _():
+            piece(r, 2 * kind + q, 6, across).wait_recv()
+
+        piece(r, 2 * kind + q, 6 + n, across).start()
+        piece(r, 2 * kind + q, 10 + n, beside).start()
+
+    half_rows = fbuf.shape[1] // 2
+    half = pl.ds(g * half_rows, half_rows)
+
+    def f_pass(c, to, sem):
+        return remote(fbuf.at[c, half], fbuf.at[c, half], fss.at[sem], fzr.at[c], to, t)
+
+    def f_swap(c):
+        return remote(fbuf.at[c, half], fbuf.at[c, half], fys.at[c], fyr.at[c], k, t, 1 - g)
+
+    def f_begin():
+        f_load.wait()
+
+        @pl.when(k < 3)
+        def _():
+            f_pass(k, k + 1, 4).start()
+
+        @pl.when(k > 0)
+        def _():
+            f_pass(k, k - 1, 5).start()
+
+    pl.when(is_end)(f_begin)
+    for q in range(2):
+        spread(far_src, 2 * q + 1, q)
+        spread(near_src, 2 * q, q)
+    pl.when(inside)(f_begin)
+    def cross_in(n, r):
+        for q in range(2):
+            piece(r, 2 - 2 * kind + q, 6, across).wait_recv()
+            piece(r, 2 - 2 * kind + q, 14 + 2 * q + n, beside).start()
+
+    def beside_in(r):
+        for q in range(4):
+            piece(r, q, 6, beside).wait_recv()
+
+    near_mate = jnp.where(k <= 1, 1 - corner, 3 - corner)
+    far_mate = jnp.where(k <= 1, 3 - corner, 1 - corner)
+    cross_in(1, far_src)
+
+    def f_forwards(c):
+        return jnp.logical_or(jnp.logical_and(c < k, k < 3), jnp.logical_and(c > k, k > 0))
+
+    def f_take(c):
+        to = jnp.where(c < k, k + 1, k - 1)
+        f_pass(c, k, c).wait_recv()
+
+        @pl.when(f_forwards(c))
+        def _():
+            f_pass(c, to, c).start()
+
+        f_swap(c).start()
+
     f_order = (jnp.where(is_end, near, end), 3 - near, 3 - end)
 
     for load in locals_[1:]:
@@ -523,9 +534,15 @@
     )
     for load in loads:
         load.wait()
-    for r in (1 - corner, 3 - corner):
-        for q in range(4):
-            piece(r, q, 6, beside).wait_recv()
+
+    @pl.when(jnp.logical_or(inside, far_mate == 3 - end))
+    def _():
+        beside_in(far_mate)
+
+    @pl.when(inside)
+    def _():
+        cross_in(0, near_src)
+        beside_in(near_mate)
 
     nt = (((1,), (1,)), ((), ()))
 
@@ -572,15 +589,16 @@
             r_scr, u_scr, c_scr, kf, vf,
         )
 
-    def accept_all():
+    def accept_some(low, high):
         def one(i, carry):
             accept(i)
             return carry
 
-        lax.fori_loop(0, blocks, one, 0)
+        lax.fori_loop(low, high, one, 0)
 
     chunk_head, chunk_stage = (0, 1, 0, 0, 2, 1, 1, 3, 2, 3, 2, 3), (0, 0, 1, 2, 0, 1, 2, 0, 1, 1, 2, 2)
     prepared = (3 - end, end, 3 - near, near)
+    late = (3 - end, end, 3 - near, near, end)
 
     def settle_small():
         few_ref[...] = esend[k]
@@ -606,7 +624,7 @@
             return carry
 
         lax.fori_loop(0, 4, one, 0)
-        accept_all()
+        accept_some(0, blocks // 2)
         f_take(f_order[0])
         f_take(f_order[1])
 
@@ -614,9 +632,19 @@
         h, stage = pick(i, chunk_head), pick(i, chunk_stage)
         r = pick(stage, (3 - end, 3 - near, near))
 
-        @pl.when(jnp.logical_and(is_end, i < 4))
-        def _():
-            prepare(pick(i, prepared))
+        @pl.when(jnp.logical_and(is_end, i == 2))
+        def _():
+            cross_in(0, near_src)
+
+            @pl.when(far_mate != 3 - end)
+            def _():
+                beside_in(far_mate)
+
+            beside_in(near_mate)
+
+        @pl.when(jnp.logical_and(is_end, jnp.logical_and(i < 5, i != 1)))
+        def _():
+            prepare(pick(i, late))
 
         @pl.when(is_end)
         def _():
@@ -629,24 +657,32 @@
             sbuf[i] = (part + from_end(i)).astype(bf16)
             remote(sbuf.at[i], bbuf.at[i], ss.at[i], br.at[i], 3 - near, t).start()
 
-        @pl.when(jnp.logical_and(inside, i == 2))
+        @pl.when(jnp.logical_and(inside, i == 0))
+        def _():
+            accept_some(blocks // 2, blocks * 2 // 3)
+
+        @pl.when(jnp.logical_and(inside, i == 1))
+        def _():
+            accept_some(blocks * 2 // 3, blocks)
+
+        @pl.when(jnp.logical_and(inside, i == 3))
         def _():
             f_take(f_order[2])
 
-        back = jnp.logical_or(jnp.logical_or(i == 2, i == 3), jnp.logical_or(i == 6, i == 9))
+        back = jnp.logical_or(jnp.logical_or(i == 3, i == 4), jnp.logical_or(i == 6, i == 9))
 
         @pl.when(jnp.logical_and(inside, back))
         def _():
-            m = jnp.where(i == 2, 0, i // 3)
+            m = jnp.where(i <= 4, i - 3, i // 3)
             part = product(end, m)
             sbuf[12 + m] = (part + from_inner(pick(m, (0, 1, 4, 7)))).astype(bf16)
             remote(sbuf.at[12 + m], cbuf.at[m], ss.at[12 + m], cr.at[m], end, t).start()
 
-        @pl.when(jnp.logical_and(inside, i == 4))
+        @pl.when(jnp.logical_and(inside, i == 5))
         def _():
             settle_small()
 
-        ready = jnp.logical_or(jnp.logical_or(i == 4, i == 7), i == 10)
+        ready = jnp.logical_or(jnp.logical_or(i == 5, i == 8), i == 10)
 
         @pl.when(jnp.logical_and(inside, ready))
         def _():
@@ -655,7 +691,7 @@
 
         for m in range(3):
 
-            @pl.when(jnp.logical_and(inside, i == 4 + 3 * m))
+            @pl.when(jnp.logical_and(inside, i == (5, 8, 10)[m]))
             def _():
                 attention(m)
 
@@ -670,7 +706,7 @@
     @pl.when(is_end)
     def _():
         f_take(f_order[0])
-        accept_all()
+        accept_some(0, blocks)
         settle_small()
         f_take(f_order[1])
 
@@ -682,7 +718,7 @@
         for m in range(3):
             acc[m] = returned(m)
             attention(m)
-            if m == 1:
+            if m == 0:
                 f_take(f_order[2])
         last[...] = returned(3)
 

time: 103 us -> 98.8 us (0.959); the launches traced: 101 us -> 98 us
  Pallas kernels: 99.4 us -> 96.6 us
    pallas_call x1, Pallas kernels: 80.1 us -> 77.9 us  [project(): pl.pallas_call(project_kernel, in_specs=[hbm] * 19, out_specs=[vmem] * 5,...]
where the time goes in v6:
time: 98.8 us; the launch traced here: 98 us
  Pallas kernels  96.6 us (98%)
    pallas_call x1, Pallas kernels, project(): pl.pallas_call(project_kernel, in_specs=[hbm] * 19, out_specs=[vmem] * 5,...  77.9 us
    pallas_call x1, Pallas kernels, mix(): pl.pallas_call(mix_kernel, in_specs=[vmem], out_specs=vmem, out_shape=jax...  13.2 us
    pallas_call x1, Pallas kernels, last_head(): pl.pallas_call(functools.partial(last_kernel, heads), in_specs=[vmem] * 6...  5.44 us

profile of v6, /device:TPU:9, one launch (start us, length us, event | category | flops | bytes accessed | tf_op | source)
XLA Modules:
  0.0 98.0 jit_solution(8769806332543971573)
XLA Ops:
  0.6 77.9 %project.1 = (f32[192,512]{1,0:T(8,128)S(1)}, f32[192,16]{1,0:T(8,128)S(1)}, f32[48,4,128,128]{3,2,1,0:T(8,128)S(1)}, bf16[4,512,1024]{2,1,0:T(8,128)(2,1)S(1)}, bf16[192,512]{1,0:T(8,128)(2,1)S(1)}) custom-call(bf16[192,1024]{1,0:T(8,128)(2,1)} %x_hbm.1, f32[4,1,1024]{2,1,0:T(1,128)} %bitcast.18, bf16[48,4,4,128]{3,2,1,0:T(4,128)(2,1)} %keys_hbm.1, ...), custom_call_target="tpu_custom_call" | custom-call | tf_op jit(solution)/shard_map/project/pallas_call | solution.py:791
  78.6 5.4 %last_head.1 = (bf16[4,192,1024]{2,1,0:T(8,128)(2,1)S(1)}, f32[48,4,128,128]{3,2,1,0:T(8,128)}) custom-call(f32[192,16]{1,0:T(8,128)S(1)} %get-tuple-element.9.thin, f32[1,128]{1,0:T(1,128)} %bitcast.26, f32[192,512]{1,0:T(8,128)S(1)} %get-tuple-element.10.parts, f32[48,4,128,128]{3,2,1,0:T(8,128)S(1)} %get-tuple-element.11.state, ...), custom_call_target="tpu_custom_call" | custom-call | flops 5000000000 | bytes 12582912 | tf_op jit(solution)/shard_map/last_head/pallas_call | solution.py:298
  84.0 13.2 %mix.1 = bf16[192,1024]{1,0:T(8,128)(2,1)S(1)} custom-call(bf16[4,192,1024]{2,1,0:T(8,128)(2,1)S(1)} %get-tuple-element.14.part), custom_call_target="tpu_custom_call" | custom-call | tf_op jit(solution)/shard_map/mix/pallas_call | solution.py:883
  97.2 0.7 copy.22

commit v7 on v6

--- a/solution.py
+++ b/solution.py
@@ -510,23 +510,7 @@
 
     near_mate = jnp.where(k <= 1, 1 - corner, 3 - corner)
     far_mate = jnp.where(k <= 1, 3 - corner, 1 - corner)
-    cross_in(1, far_src)
-
-    def f_forwards(c):
-        return jnp.logical_or(jnp.logical_and(c < k, k < 3), jnp.logical_and(c > k, k > 0))
-
-    def f_take(c):
-        to = jnp.where(c < k, k + 1, k - 1)
-        f_pass(c, k, c).wait_recv()
-
-        @pl.when(f_forwards(c))
-        def _():
-            f_pass(c, to, c).start()
-
-        f_swap(c).start()
-
-    f_order = (jnp.where(is_end, near, end), 3 - near, 3 - end)
-
+    lazy = jnp.logical_and(is_end, far_mate == 3 - end)
     for load in locals_[1:]:
         load.wait()
     thin[...] = rows_to_columns(
@@ -534,6 +518,26 @@
     )
     for load in loads:
         load.wait()
+
+    @pl.when(jnp.logical_not(lazy))
+    def _():
+        cross_in(1, far_src)
+
+
+    def f_forwards(c):
+        return jnp.logical_or(jnp.logical_and(c < k, k < 3), jnp.logical_and(c > k, k > 0))
+
+    def f_take(c):
+        to = jnp.where(c < k, k + 1, k - 1)
+        f_pass(c, k, c).wait_recv()
+
+        @pl.when(f_forwards(c))
+        def _():
+            f_pass(c, to, c).start()
+
+        f_swap(c).start()
+
+    f_order = (jnp.where(is_end, near, end), 3 - near, 3 - end)
 
     @pl.when(jnp.logical_or(inside, far_mate == 3 - end))
     def _():
@@ -624,8 +628,8 @@
             return carry
 
         lax.fori_loop(0, 4, one, 0)
+        f_take(f_order[0])
         accept_some(0, blocks // 2)
-        f_take(f_order[0])
         f_take(f_order[1])
 
     def step(i, carry):
@@ -634,6 +638,7 @@
 
         @pl.when(jnp.logical_and(is_end, i == 2))
         def _():
+            pl.when(lazy)(lambda: cross_in(1, far_src))
             cross_in(0, near_src)
 
             @pl.when(far_mate != 3 - end)

time: 98.8 us -> 97.7 us (0.989)
  no operation moved by 1% of the time
where the time goes in v7:
time: 97.7 us; the launch traced here: 97.4 us
  Pallas kernels  96 us (98%)
    pallas_call x1, Pallas kernels, project(): pl.pallas_call(project_kernel, in_specs=[hbm] * 19, out_specs=[vmem] * 5,...  77.9 us
    pallas_call x1, Pallas kernels, mix(): pl.pallas_call(mix_kernel, in_specs=[vmem], out_specs=vmem, out_shape=jax...  12.7 us
    pallas_call x1, Pallas kernels, last_head(): pl.pallas_call(functools.partial(last_kernel, heads), in_specs=[vmem] * 6...  5.44 us

profile of v7, /device:TPU:9, one launch (start us, length us, event | category | flops | bytes accessed | tf_op | source)
XLA Modules:
  0.0 97.4 jit_solution(12654894717316161475)
XLA Ops:
  0.6 77.9 %project.1 = (f32[192,512]{1,0:T(8,128)S(1)}, f32[192,16]{1,0:T(8,128)S(1)}, f32[48,4,128,128]{3,2,1,0:T(8,128)S(1)}, bf16[4,512,1024]{2,1,0:T(8,128)(2,1)S(1)}, bf16[192,512]{1,0:T(8,128)(2,1)S(1)}) custom-call(bf16[192,1024]{1,0:T(8,128)(2,1)} %x_hbm.1, f32[4,1,1024]{2,1,0:T(1,128)} %bitcast.18, bf16[48,4,4,128]{3,2,1,0:T(4,128)(2,1)} %keys_hbm.1, ...), custom_call_target="tpu_custom_call" | custom-call | tf_op jit(solution)/shard_map/project/pallas_call | solution.py:796
  78.6 5.4 %last_head.1 = (bf16[4,192,1024]{2,1,0:T(8,128)(2,1)S(1)}, f32[48,4,128,128]{3,2,1,0:T(8,128)}) custom-call(f32[192,16]{1,0:T(8,128)S(1)} %get-tuple-element.9.thin, f32[1,128]{1,0:T(1,128)} %bitcast.26, f32[192,512]{1,0:T(8,128)S(1)} %get-tuple-element.10.parts, f32[48,4,128,128]{3,2,1,0:T(8,128)S(1)} %get-tuple-element.11.state, ...), custom_call_target="tpu_custom_call" | custom-call | flops 5000000000 | bytes 12582912 | tf_op jit(solution)/shard_map/last_head/pallas_call | solution.py:298
  84.0 12.7 %mix.1 = bf16[192,1024]{1,0:T(8,128)(2,1)S(1)} custom-call(bf16[4,192,1024]{2,1,0:T(8,128)(2,1)S(1)} %get-tuple-element.14.part), custom_call_target="tpu_custom_call" | custom-call | tf_op jit(solution)/shard_map/mix/pallas_call | solution.py:888
  96.7 0.7 copy.22

commit v8 on v7

--- a/solution.py
+++ b/solution.py
@@ -198,6 +198,7 @@
 
 
 GROUP = 3
+COPIES = 8
 
 
 def attend_head(h, heads, blocks, scratch, parts_at, thin, state, gain, flat):
@@ -226,8 +227,13 @@
 
 def last_kernel(heads, thin, w_ref, parts, state, some, columns, o_ref, kept, flat, *rest):
     scratch, done = rest[:-1], rest[-1]
-    keep = pltpu.make_async_copy(state, kept, done)
-    keep.start()
+    span = state.shape[0] // COPIES
+    keeps = [
+        pltpu.make_async_copy(state.at[pl.ds(n * span, span)], kept.at[pl.ds(n * span, span)], done.at[n])
+        for n in range(COPIES)
+    ]
+    for keep in keeps:
+        keep.start()
     flat[...] = some[...]
     blocks = state.shape[0] // SB
     attend_head(
@@ -235,7 +241,8 @@
     )
     for c in range(columns.shape[0]):
         o_ref[c] = jnp.dot(flat[...], columns[c], preferred_element_type=f32).astype(bf16)
-    keep.wait()
+    for keep in keeps:
+        keep.wait()
 
 
 def accepted(state, keys, values, few):
@@ -306,7 +313,7 @@
         scratch_shapes=[
             pltpu.VMEM((rows, width), bf16),
             *[pltpu.VMEM((GROUP * TALL, DK), f32)] * 7,
-            pltpu.SemaphoreType.DMA,
+            pltpu.SemaphoreType.DMA((COPIES,)),
         ],
         compiler_params=pltpu.CompilerParams(vmem_limit_bytes=LIMIT),
         cost_estimate=pl.CostEstimate(flops=5_000_000_000, bytes_accessed=state.size * 4, transcendentals=0),
@@ -674,11 +681,11 @@
         def _():
             f_take(f_order[2])
 
-        back = jnp.logical_or(jnp.logical_or(i == 3, i == 4), jnp.logical_or(i == 6, i == 9))
+        back = jnp.logical_or(jnp.logical_or(i == 4, i == 5), jnp.logical_or(i == 7, i == 9))
 
         @pl.when(jnp.logical_and(inside, back))
         def _():
-            m = jnp.where(i <= 4, i - 3, i // 3)
+            m = jnp.where(i <= 5, i - 4, jnp.where(i == 7, 2, 3))
             part = product(end, m)
             sbuf[12 + m] = (part + from_inner(pick(m, (0, 1, 4, 7)))).astype(bf16)
             remote(sbuf.at[12 + m], cbuf.at[m], ss.at[12 + m], cr.at[m], end, t).start()

time: 97.7 us -> 97.5 us (level)
  no operation moved by 1% of the time
where the time goes in v8:
time: 97.5 us; the launch traced here: 97.3 us
  Pallas kernels  95.9 us (98%)
    pallas_call x1, Pallas kernels, project(): pl.pallas_call(project_kernel, in_specs=[hbm] * 19, out_specs=[vmem] * 5,...  77.9 us
    pallas_call x1, Pallas kernels, mix(): pl.pallas_call(mix_kernel, in_specs=[vmem], out_specs=vmem, out_shape=jax...  12.7 us
    pallas_call x1, Pallas kernels, last_head(): pl.pallas_call(functools.partial(last_kernel, heads), in_specs=[vmem] * 6...  5.31 us

profile of v8, /device:TPU:9, one launch (start us, length us, event | category | flops | bytes accessed | tf_op | source)
XLA Modules:
  0.0 97.3 jit_solution(9931039435715512825)
XLA Ops:
  0.6 77.9 %project.1 = (f32[192,512]{1,0:T(8,128)S(1)}, f32[192,16]{1,0:T(8,128)S(1)}, f32[48,4,128,128]{3,2,1,0:T(8,128)S(1)}, bf16[4,512,1024]{2,1,0:T(8,128)(2,1)S(1)}, bf16[192,512]{1,0:T(8,128)(2,1)S(1)}) custom-call(bf16[192,1024]{1,0:T(8,128)(2,1)} %x_hbm.1, f32[4,1,1024]{2,1,0:T(1,128)} %bitcast.18, bf16[48,4,4,128]{3,2,1,0:T(4,128)(2,1)} %keys_hbm.1, ...), custom_call_target="tpu_custom_call" | custom-call | tf_op jit(solution)/shard_map/project/pallas_call | solution.py:803
  78.6 5.3 %last_head.1 = (bf16[4,192,1024]{2,1,0:T(8,128)(2,1)S(1)}, f32[48,4,128,128]{3,2,1,0:T(8,128)}) custom-call(f32[192,16]{1,0:T(8,128)S(1)} %get-tuple-element.9.thin, f32[1,128]{1,0:T(1,128)} %bitcast.26, f32[192,512]{1,0:T(8,128)S(1)} %get-tuple-element.10.parts, f32[48,4,128,128]{3,2,1,0:T(8,128)S(1)} %get-tuple-element.11.state, ...), custom_call_target="tpu_custom_call" | custom-call | flops 5000000000 | bytes 12582912 | tf_op jit(solution)/shard_map/last_head/pallas_call | solution.py:305
  83.9 12.7 %mix.1 = bf16[192,1024]{1,0:T(8,128)(2,1)S(1)} custom-call(bf16[4,192,1024]{2,1,0:T(8,128)(2,1)S(1)} %get-tuple-element.14.part), custom_call_target="tpu_custom_call" | custom-call | tf_op jit(solution)/shard_map/mix/pallas_call | solution.py:895
  96.6 0.7 copy.22
